TPU v7x, 32 devices: a whole 2x2x4 slice. The times are simulated.
32 devices in a mesh: grp: 2 (over y), tp: 4 (over z), dp: 4 (over x, core).
Axes of the slice: x: 2, y: 2, z: 4, core: 2. Of those that a mesh axis runs over, the one named last changes fastest.
Arguments:
- tokens: bfloat16 [128, 8, 2048], P('grp', None, 'dp'), parts along dimension 0, may hold values from -64 to 64
- live_counts: int32 [128], P(('grp', 'dp')), parts along dimension 0, may hold values from 1 to 8, 256 in all
- norm_gain: float32 [2, 2048], P(None, 'dp'), may hold values from 0.1 to 1.9
- w_branch: bfloat16 [2, 2048, 4096], P(None, 'dp', 'tp'), may hold values from -0.125 to 0.125
- w_silu_gate: bfloat16 [2, 2048, 4096], P(None, 'dp', 'tp'), may hold values from -0.125 to 0.125
- conv_weight: float32 [2, 4, 4096], P(None, None, 'tp'), may hold values from -3 to 3
- w_query: bfloat16 [2, 16, 256, 256], P(None, 'tp'), may hold values from -0.375 to 0.375
- w_key: bfloat16 [2, 16, 256, 256], P(None, 'tp'), may hold values from -0.375 to 0.375
- w_value: bfloat16 [2, 16, 256, 256], P(None, 'tp'), may hold values from -0.375 to 0.375
- w_input_gate: bfloat16 [2, 16, 768], P(None, 'tp'), may hold values from -0.21875 to 0.21875
- w_forget_gate: bfloat16 [2, 16, 768], P(None, 'tp'), may hold values from -0.21875 to 0.21875
- bias_input: float32 [2, 16], P(None, 'tp'), may hold values from -2 to 2
- bias_forget: float32 [2, 16], P(None, 'tp'), may hold values from -1 to 5
- out_gain: float32 [2, 16, 256], P(None, 'tp'), may hold values from 0.25 to 4
- skip_gain: float32 [2, 4096], P(None, 'tp'), may hold values from 0.25 to 4
- w_out: bfloat16 [2, 4096, 2048], P(None, 'tp', 'dp'), may hold values from -0.09375 to 0.09375
- conv_state: bfloat16 [2, 128, 3, 4096], P(None, ('grp', 'dp'), None, 'tp'), parts along dimension 1, may hold values from -6 to 6
- memory: float32 [2, 128, 16, 256, 256], P(None, ('grp', 'dp'), 'tp'), parts along dimension 1, may hold values from -0.375 to 0.375
- max_state: float32 [2, 128, 16], P(None, ('grp', 'dp'), 'tp'), parts along dimension 1, may hold values from -4 to 4
Outputs:
- out_tokens: bfloat16 [128, 8, 2048], P('grp', None, 'dp'), parts along dimension 0
- new_conv_state: bfloat16 [2, 128, 3, 4096], P(None, ('grp', 'dp'), None, 'tp'), parts along dimension 1
- new_memory: float32 [2, 128, 16, 256, 256], P(None, ('grp', 'dp'), 'tp'), parts along dimension 1
- new_max: float32 [2, 128, 16], P(None, ('grp', 'dp'), 'tp'), parts along dimension 1
There are 2 independent parts, one for each index of `grp`. A program takes and returns all parts, laid end to end along the dimension named above; an argument that names none is the same for every part. Nothing has to cross between parts.
Inputs may be any that keep to these rules, and one draw needn't show every extreme that they name: `live_counts`: each sequence has at least one live slot; within each part (each independent copy of the problem) the 64 counts sum to 256, so the whole array sums to that times the number of parts; in each part some sequence uses all 8 slots.
All inputs are finite; a program needn't handle non-finite values. No bound on the sum of `live_counts` on one device may be relied on, other than what follows from the above.
Results may differ from a plain program's by a relative error of at most 0.035.
Values may be sent and summed in bfloat16 or wider, within the bound.
A program may use at most 192 MiB of HBM per device.

v0:
```python
import functools

import jax
import jax.numpy as jnp
from jax import lax
from jax.experimental import pallas as pl
from jax.experimental.pallas import tpu as pltpu
from jax.sharding import PartitionSpec as P

HEAD_DIM = 256
CONV = 4
LAYERS = 2
epsilon = 1e-06
very_negative = -1e30

VM = pl.BlockSpec(memory_space=pltpu.VMEM)
MESH = pl.DeviceIdType.MESH


def greet(axis, devices):
    barrier = pltpu.get_barrier_semaphore()
    for device in devices:
        pl.semaphore_signal(barrier, inc=1, device_id={axis: device}, device_id_type=MESH)
    pl.semaphore_wait(barrier, len(devices))


def rcopy(src, dst, send, recv, axis, device):
    return pltpu.make_async_remote_copy(
        src_ref=src, dst_ref=dst, send_sem=send, recv_sem=recv,
        device_id={axis: device}, device_id_type=MESH,
    )


def scatter_kernel(n, chunks, a_ref, b_ref, aux_ref, oa_ref, ob_ref, oaux_ref,
                   r1a, r1b, s2a, s2b, r2a, r2b, s1s, s1r, s2s, s2r, axs, axr):
    nx = n // 2
    me = lax.axis_index("dp")
    core = me % 2
    x = me // 2
    partner = me + 1 - 2 * core
    greet("dp", [(me + off) % n for off in range(1, n)])
    started = []
    aux_copies = []
    first = {}
    for g in range(nx):
        xo = (x + 1 + g) % nx
        for c in range(chunks):
            pair = []
            for k, (src, dst) in enumerate(((a_ref, r1a), (b_ref, r1b))):
                cp = rcopy(src.at[xo, 1 - core, c], dst.at[g, c],
                           s1s.at[g, c, k], s1r.at[g, c, k], "dp", partner)
                cp.start()
                pair.append(cp)
                started.append(cp)
            first[g, c] = pair
        if g == 0:
            for off in range(1, n):
                to = (me + off) % n
                cp = rcopy(aux_ref.at[to], oaux_ref.at[me], axs.at[off - 1], axr.at[off - 1], "dp", to)
                cp.start()
                aux_copies.append(cp)
                started.append(cp)
            oaux_ref[me] = aux_ref[me]
    second = {}
    for g in range(nx - 1):
        xo = (x + 1 + g) % nx
        for c in range(chunks):
            pair = []
            for k, (src, got, buf, dst) in enumerate(((a_ref, r1a, s2a, r2a), (b_ref, r1b, s2b, r2b))):
                first[g, c][k].wait_recv()
                buf[g, c] = (
                    src[xo, core, c].astype(jnp.float32) + got[g, c].astype(jnp.float32)
                ).astype(jnp.bfloat16)
                cp = rcopy(buf.at[g, c], dst.at[g, c], s2s.at[g, c, k], s2r.at[g, c, k],
                           "dp", 2 * xo + core)
                cp.start()
                pair.append(cp)
                started.append(cp)
            second[g, c] = pair
    for c in range(chunks):
        for k, (src, got, more, out) in enumerate(((a_ref, r1a, r2a, oa_ref), (b_ref, r1b, r2b, ob_ref))):
            first[nx - 1, c][k].wait_recv()
            total = src[x, core, c].astype(jnp.float32) + got[nx - 1, c].astype(jnp.float32)
            for g in range(nx - 1):
                second[g, c][k].wait_recv()
                total = total + more[g, c].astype(jnp.float32)
            out[c] = total
    for cp in aux_copies:
        cp.wait_recv()
    for cp in started:
        cp.wait_send()


def scatter_dp(n, a, b, aux):
    rows, width = a.shape
    nx = n // 2
    own = rows // n
    chunks = 4 if own % 64 == 0 else 1
    piece = own // chunks
    a = a.reshape(nx, 2, chunks, piece, width)
    b = b.reshape(nx, 2, chunks, piece, width)
    far = max(nx - 1, 1)
    bf = jnp.bfloat16
    sem = pltpu.SemaphoreType.DMA
    oa, ob, oaux = pl.pallas_call(
        functools.partial(scatter_kernel, n, chunks),
        out_shape=(
            jax.ShapeDtypeStruct((chunks, piece, width), jnp.float32),
            jax.ShapeDtypeStruct((chunks, piece, width), jnp.float32),
            jax.ShapeDtypeStruct(aux.shape, jnp.float32),
        ),
        in_specs=[VM] * 3,
        out_specs=(VM,) * 3,
        scratch_shapes=[
            pltpu.VMEM((nx, chunks, piece, width), bf),
            pltpu.VMEM((nx, chunks, piece, width), bf),
            pltpu.VMEM((far, chunks, piece, width), bf),
            pltpu.VMEM((far, chunks, piece, width), bf),
            pltpu.VMEM((far, chunks, piece, width), bf),
            pltpu.VMEM((far, chunks, piece, width), bf),
            sem((nx, chunks, 2)), sem((nx, chunks, 2)),
            sem((far, chunks, 2)), sem((far, chunks, 2)),
            sem((n - 1,)), sem((n - 1,)),
        ],
        compiler_params=pltpu.CompilerParams(collective_id=0, has_side_effects=True),
        name="scatter_dp",
    )(a, b, aux)
    return oa.reshape(own, width), ob.reshape(own, width), oaux


def gather_kernel(n, chunks, m_ref, out_ref, xs, xr, ps, pr, fs, fr):
    nx = n // 2
    me = lax.axis_index("dp")
    core = me % 2
    x = me // 2
    partner = me + 1 - 2 * core
    greet("dp", [partner] + [2 * ((x + 1 + g) % nx) + core for g in range(nx - 1)])
    started = []
    across = {}
    near = {}
    for c in range(chunks):
        for g in range(nx - 1):
            to = 2 * ((x + 1 + g) % nx) + core
            cp = rcopy(m_ref.at[c], out_ref.at[x, core, c], xs.at[g, c], xr.at[g, c], "dp", to)
            cp.start()
            across[g, c] = cp
            started.append(cp)
    for c in range(chunks):
        cp = rcopy(m_ref.at[c], out_ref.at[x, core, c], ps.at[c], pr.at[c], "dp", partner)
        cp.start()
        near[c] = cp
        started.append(cp)
    out_ref[x, core] = m_ref[...]
    passed = []
    for c in range(chunks):
        for g in range(nx - 1):
            origin = (x + nx - 1 - g) % nx
            across[g, c].wait_recv()
            cp = rcopy(out_ref.at[origin, core, c], out_ref.at[origin, core, c],
                       fs.at[g, c], fr.at[g, c], "dp", partner)
            cp.start()
            passed.append(cp)
            started.append(cp)
    for c in range(chunks):
        near[c].wait_recv()
    for cp in passed:
        cp.wait_recv()
    for cp in started:
        cp.wait_send()


def gather_dp(n, m):
    own, width = m.shape
    nx = n // 2
    chunks = 4 if own % 64 == 0 else 1
    piece = own // chunks
    far = max(nx - 1, 1)
    sem = pltpu.SemaphoreType.DMA
    out = pl.pallas_call(
        functools.partial(gather_kernel, n, chunks),
        out_shape=jax.ShapeDtypeStruct((nx, 2, chunks, piece, width), m.dtype),
        in_specs=[VM],
        out_specs=VM,
        scratch_shapes=[
            sem((far, chunks)), sem((far, chunks)), sem((chunks,)), sem((chunks,)),
            sem((far, chunks)), sem((far, chunks)),
        ],
        compiler_params=pltpu.CompilerParams(collective_id=1, has_side_effects=True),
        name="gather_dp",
    )(m.reshape(chunks, piece, width))
    return out.reshape(n * own, width)


def reduce_kernel(n, p_ref, x_ref, out_ref, got, mine, s1, r1, s2, r2):
    me = lax.axis_index("tp")
    greet("tp", [(me + off) % n for off in range(1, n)])
    started = []
    first = []
    order = sorted(range(1, n), key=lambda off: -min(off, n - off))
    for off in order:
        to = (me + off) % n
        cp = rcopy(p_ref.at[to], got.at[off - 1], s1.at[off - 1], r1.at[off - 1], "tp", to)
        cp.start()
        started.append(cp)
        first.append((off, cp))
    total = p_ref[me].astype(jnp.float32)
    for off, cp in first:
        cp.wait_recv()
        total = total + got[off - 1].astype(jnp.float32)
    update = total.astype(jnp.bfloat16).astype(jnp.float32)
    mine[...] = (x_ref[me].astype(jnp.float32) + update).astype(jnp.bfloat16)
    second = []
    for off in order:
        to = (me + off) % n
        cp = rcopy(mine, out_ref.at[me], s2.at[off - 1], r2.at[off - 1], "tp", to)
        cp.start()
        started.append(cp)
        second.append(cp)
    out_ref[me] = mine[...]
    for cp in second:
        cp.wait_recv()
    for cp in started:
        cp.wait_send()


def reduce_tp(n, p, x):
    rows, width = p.shape
    share = rows // n
    sem = pltpu.SemaphoreType.DMA
    out = pl.pallas_call(
        functools.partial(reduce_kernel, n),
        out_shape=jax.ShapeDtypeStruct((n, share, width), jnp.bfloat16),
        in_specs=[VM] * 2,
        out_specs=VM,
        scratch_shapes=[
            pltpu.VMEM((n - 1, share, width), jnp.bfloat16),
            pltpu.VMEM((share, width), jnp.bfloat16),
            sem((n - 1,)), sem((n - 1,)), sem((n - 1,)), sem((n - 1,)),
        ],
        compiler_params=pltpu.CompilerParams(collective_id=2, has_side_effects=True),
        name="reduce_tp",
    )(p.reshape(n, share, width), x.reshape(n, share, width))
    return out.reshape(rows, width)


def cell_kernel(heads, q_ref, k_ref, v_ref, w_ref, s_ref, c_ref, *rest):
    num_ref, new_ref = rest[-2:]
    for h in range(heads):
        q = q_ref[0, h]
        k = k_ref[0, h]
        v = v_ref[0, h]
        scal = s_ref[0, h]
        old = c_ref[0, 0, h]
        scores = lax.dot_general(q, k, (((1,), (1,)), ((), ())), preferred_element_type=jnp.float32)
        scores = scores * w_ref[0, h]
        inside = jnp.dot(scores, v, preferred_element_type=jnp.float32)
        carried = jnp.dot(
            q.astype(jnp.bfloat16), old.astype(jnp.bfloat16), preferred_element_type=jnp.float32
        )
        num_ref[0, h] = inside + scal[:, 0:1] * carried
        outer = lax.dot_general(
            k * scal[:, 1:2], v, (((0,), (0,)), ((), ())), preferred_element_type=jnp.float32
        )
        new_ref[0, 0, h] = scal[0:1, 2:3] * old + outer


def memory_cell(layer, q, k, v, weights, scal, memory, previous):
    batch, heads, steps, dim = q.shape
    row = pl.BlockSpec((1, heads, steps, dim), lambda b: (b, 0, 0, 0))
    small = pl.BlockSpec((1, heads, steps, steps), lambda b: (b, 0, 0, 0))
    three = pl.BlockSpec((1, heads, steps, 3), lambda b: (b, 0, 0, 0))
    mat = pl.BlockSpec((1, 1, heads, dim, dim), lambda b: (layer, b, 0, 0, 0))
    args = [q, k, v, weights, scal, memory]
    specs = [row, row, row, small, three, mat]
    aliases = {}
    if previous is not None:
        args.append(previous)
        specs.append(pl.BlockSpec(memory_space=pl.ANY))
        aliases = {6: 1}
    return pl.pallas_call(
        functools.partial(cell_kernel, heads),
        grid=(batch,),
        out_shape=(
            jax.ShapeDtypeStruct(q.shape, jnp.float32),
            jax.ShapeDtypeStruct(memory.shape, jnp.float32),
        ),
        in_specs=specs,
        out_specs=(row, mat),
        input_output_aliases=aliases,
        compiler_params=pltpu.CompilerParams(dimension_semantics=("arbitrary",)),
        name="memory_cell",
    )(*args)


def per_device(tokens, live_counts, norm_gain, w_branch, w_silu_gate, conv_weight, w_query, w_key,
               w_value, w_input_gate, w_forget_gate, bias_input, bias_forget, out_gain, skip_gain,
               w_out, conv_state, memory, max_state):
    f32 = jnp.float32
    bf = jnp.bfloat16
    ndp = lax.axis_size("dp")
    ntp = lax.axis_size("tp")
    all_batch, steps, features = tokens.shape
    batch = live_counts.shape[0]
    width = w_branch.shape[2]
    heads = w_query.shape[1]
    rows = all_batch * steps
    own = batch * steps
    live_rows = all_batch * steps // 2
    lanes = -(-own // 128) * 128
    model = features * ndp
    flat_tokens = tokens.reshape(rows, features)
    positions = jnp.arange(steps, dtype=jnp.int32)
    live = positions[None, :] < live_counts[:, None]
    causal = positions[:, None] >= positions[None, :]
    picks = live_counts[:, None] + jnp.arange(CONV - 1, dtype=jnp.int32)[None, :]
    pick_hot = picks[:, :, None] == jnp.arange(steps + CONV - 1, dtype=jnp.int32)[None, None, :]
    count_row = jnp.pad(live_counts.astype(f32), (0, lanes - batch))

    dense = flat_tokens
    compact = None
    select = None
    live_all = None
    new_memory = None
    conv_list = []
    max_list = []
    for l in range(LAYERS):
        floats = dense.astype(f32)
        squares = jnp.sum(floats * floats, axis=-1).reshape(ndp, own)
        squares = jnp.pad(squares, ((0, 0), (0, lanes - own)))
        aux = jnp.stack([squares, jnp.broadcast_to(count_row, squares.shape)], axis=1)
        aux = jnp.pad(aux, ((0, 0), (0, 6), (0, 0)))
        scaled = (floats * norm_gain[l]).astype(bf)
        first = jnp.dot(scaled, w_branch[l], preferred_element_type=f32).astype(bf)
        second = jnp.dot(scaled, w_silu_gate[l], preferred_element_type=f32).astype(bf)
        branch, gate, aux = scatter_dp(ndp, first, second, aux)
        total = jnp.sum(aux[:, 0, :own], axis=0)
        inv = lax.rsqrt(total / model + epsilon)[:, None]
        branch = (branch * inv).astype(bf).reshape(batch, steps, width)
        gate = (gate * inv).astype(bf).astype(f32).reshape(batch, steps, width)
        if select is None:
            counts = aux[:, 1, :batch].astype(jnp.int32).reshape(all_batch)
            ids = jnp.arange(all_batch)
            before = jnp.sum(jnp.where(ids[None, :] < ids[:, None], counts[None, :], 0), axis=1)
            live_all = positions[None, :] < counts[:, None]
            place = jnp.where(live_all, before[:, None] + positions[None, :], -1).reshape(rows)
            select = (jnp.arange(live_rows)[:, None] == place[None, :]).astype(bf)
            compact = jnp.dot(select, flat_tokens, preferred_element_type=f32).astype(bf)

        padded = jnp.concatenate([conv_state[l], branch], axis=1).astype(f32)
        conv_sum = padded[:, 0:steps] * conv_weight[l, 0]
        for j in range(1, CONV):
            conv_sum = conv_sum + padded[:, j:j + steps] * conv_weight[l, j]
        convolved = jax.nn.silu(conv_sum).astype(bf)
        new_conv = jnp.stack(
            [jnp.sum(jnp.where(pick_hot[:, i, :, None], padded, 0.0), axis=1) for i in range(CONV - 1)],
            axis=1,
        ).astype(bf)
        conv_list.append(new_conv)
        conv_flat = convolved.reshape(own, width)
        branch_flat = branch.reshape(own, width)

        def project(source, w):
            parts = [
                jnp.dot(source[:, h * HEAD_DIM:(h + 1) * HEAD_DIM], w[h], preferred_element_type=f32)
                for h in range(heads)
            ]
            out = jnp.stack([p.reshape(batch, steps, HEAD_DIM) for p in parts], axis=1)
            return out.astype(bf).astype(f32)

        q = project(conv_flat, w_query[l])
        k = project(conv_flat, w_key[l])
        v = project(branch_flat, w_value[l])

        def gate_dot(w, bias):
            w = w.astype(f32).reshape(heads, 3, 1, HEAD_DIM)
            return jnp.sum(q * w[:, 0] + k * w[:, 1] + v * w[:, 2], axis=-1) + bias[:, None]

        live_h = live[:, None, :]
        ig = jnp.where(live_h, gate_dot(w_input_gate[l], bias_input[l]), very_negative)
        fg = jnp.where(live_h, jax.nn.log_sigmoid(gate_dot(w_forget_gate[l], bias_forget[l])), 0.0)
        cum = jnp.sum(jnp.where(causal, fg[..., None, :], 0.0), axis=-1)
        logw = cum[..., :, None] - cum[..., None, :] + ig[..., None, :]
        logw = jnp.where(causal, logw, very_negative)
        carried = cum + max_state[l][..., None]
        stab = jnp.maximum(jnp.max(logw, axis=-1), carried)
        weights = jnp.exp(logw - stab[..., None])
        new_max = stab[..., -1]
        decay = jnp.exp(cum[..., -1] + max_state[l] - new_max)
        upd = jnp.exp(cum[..., -1:] - cum + ig - new_max[..., None])
        scal = jnp.stack(
            [jnp.exp(carried - stab), upd, jnp.broadcast_to(decay[..., None], upd.shape)], axis=-1
        )
        max_list.append(new_max)
        num, new_memory = memory_cell(
            l, q, k * HEAD_DIM ** (-0.5), v, weights, scal, memory, new_memory
        )
        centered = num - jnp.mean(num, axis=-1, keepdims=True)
        normalized = centered * lax.rsqrt(
            jnp.mean(centered * centered, axis=-1, keepdims=True) + epsilon
        )
        normalized = normalized * out_gain[l][None, :, None, :]
        readout = jnp.transpose(normalized, (0, 2, 1, 3)).reshape(batch, steps, width)
        mixed = (readout + skip_gain[l] * convolved.astype(f32)) * jax.nn.silu(gate)
        mixed = jnp.where(live[:, :, None], mixed, 0.0).astype(bf).reshape(own, width)
        everyone = gather_dp(ndp, mixed)
        packed = jnp.dot(select, everyone, preferred_element_type=f32).astype(bf)
        part = jnp.dot(packed, w_out[l], preferred_element_type=f32).astype(bf)
        compact = reduce_tp(ntp, part, compact)
        dense = lax.dot_general(
            select, compact, (((0,), (0,)), ((), ())), preferred_element_type=f32
        ).astype(bf)
    result = jnp.where(live_all[:, :, None], dense.reshape(tokens.shape), tokens)
    return (result, jnp.stack(conv_list), new_memory, jnp.stack(max_list))


def solution(mesh):
    in_specs = (
        P("grp", None, "dp"),
        P(("grp", "dp")),
        P(None, "dp"),
        P(None, "dp", "tp"),
        P(None, "dp", "tp"),
        P(None, None, "tp"),
        P(None, "tp", None, None),
        P(None, "tp", None, None),
        P(None, "tp", None, None),
        P(None, "tp", None),
        P(None, "tp", None),
        P(None, "tp"),
        P(None, "tp"),
        P(None, "tp", None),
        P(None, "tp"),
        P(None, "tp", "dp"),
        P(None, ("grp", "dp"), None, "tp"),
        P(None, ("grp", "dp"), "tp", None, None),
        P(None, ("grp", "dp"), "tp"),
    )
    out_specs = (
        P("grp", None, "dp"),
        P(None, ("grp", "dp"), None, "tp"),
        P(None, ("grp", "dp"), "tp", None, None),
        P(None, ("grp", "dp"), "tp"),
    )
    return jax.shard_map(
        per_device, mesh=mesh, in_specs=in_specs, out_specs=out_specs, check_vma=False
    )
```

profile of v0, /device:TPU:0, one launch (start us, length us, event | category | flops | bytes accessed | tf_op | source)
XLA Modules:
  0.0 201.1 jit_solution(12372474992132130793)
XLA Ops:
  1.5 3.1 %convolution_convert_fusion.3 = bf16[512,1024]{1,0:T(8,128)(2,1)} fusion(bf16[2,512,1024]{2,1,0:T(8,128)(2,1)} %param.22, bf16[64,8,512]{2,1,0:T(8,128)(2,1)} %param.19, f32[512]{0:T(512)S(1)} %bitcast.491), kind=kOutput, calls=%fused_computation.3 | convolution fusion | flops 538181632 | bytes 2623488 | tf_op jit(solution)/shard_map/dot_general | solution.py:333
  4.6 1.7 convolution_convert_fusion.2
  7.2 19.5 %scatter_dp.2 = (f32[4,32,1024]{2,1,0:T(8,128)}, f32[4,32,1024]{2,1,0:T(8,128)}, f32[4,8,128]{2,1,0:T(8,128)}) custom-call(bf16[2,2,4,32,1024]{4,3,2,1,0:T(8,128)(2,1)} %bitcast.443, bf16[2,2,4,32,1024]{4,3,2,1,0:T(8,128)(2,1)} %bitcast.444, f32[4,8,128]{2,1,0:T(8,128)} %pad.12.aux_ref), custom_call_target="tpu_custom_call" | custom-call | tf_op jit(solution)/shard_map/scatter_dp/pallas_call | solution.py:105
  27.5 1.1 multiply_convert_fusion.5
  32.6 1.0 fusion.58
  35.3 1.0 copy.141.s_ref
  37.2 1.0 maximum_convert_fusion
  38.3 21.5 %memory_cell.2 = (f32[16,4,8,256]{3,2,1,0:T(8,128)}, f32[2,16,4,256,256]{4,3,2,1,0:T(8,128)}) custom-call(f32[16,4,8,256]{3,2,1,0:T(8,128)} %get-tuple-element.90.q_ref, f32[16,4,8,256]{3,2,1,0:T(8,128)} %get-tuple-element.36.k_ref, f32[16,4,8,256]{3,2,1,0:T(8,128)} %get-tuple-element.91.v_ref, f32[16,4,8,8]{3,2,1,0:T(8,128)} %subtract_exponential_fusion.1.w_ref, ...), custom_call_target="tpu_custom_call" | custom-call | tf_op jit(solution)/shard_map/memory_cell/pallas_call | solution.py:280
  59.8 1.3 reduce_sum.205
  61.1 1.3 multiply_reduce_fusion.1
  62.4 1.2 multiply_multiply_fusion.1
  63.7 1.2 fusion.79
  65.0 12.1 %gather_dp.2 = bf16[2,2,4,32,1024]{4,3,2,1,0:T(8,128)(2,1)} custom-call(bf16[4,32,1024]{2,1,0:T(8,128)(2,1)} %bitcast.440), custom_call_target="tpu_custom_call" | custom-call | tf_op jit(solution)/shard_map/gather_dp/pallas_call | solution.py:179
  78.2 3.0 %fusion.4 = bf16[256,512]{1,0:T(8,128)(2,1)} fusion(bf16[512,1024]{1,0:T(8,128)(2,1)} %bitcast.441, bf16[2,1024,512]{2,1,0:T(8,128)(2,1)} %param.34, s32[512]{0:T(512)S(1)} %select_n.124), kind=kOutput, calls=%fused_computation.16 | convolution fusion | flops 537395200 | bytes 2361344 | tf_op jit(solution)/shard_map/dot_general | solution.py:407
  81.2 1.0 convolution_convert_fusion.8
  82.2 18.4 %reduce_tp.2.x_ref = bf16[4,64,512]{2,1,0:T(8,128)(2,1)} custom-call(bf16[4,64,512]{2,1,0:T(8,128)(2,1)} %bitcast.450, bf16[4,64,512]{2,1,0:T(8,128)(2,1)} %bitcast.452), custom_call_target="tpu_custom_call" | custom-call | tf_op jit(solution)/shard_map/reduce_tp/pallas_call | solution.py:230
  100.6 1.5 fusion.33
  102.1 3.1 %convolution_convert_fusion = bf16[512,1024]{1,0:T(8,128)(2,1)} fusion(bf16[2,512,1024]{2,1,0:T(8,128)(2,1)} %param.23, bf16[512,512]{0,1:T(8,128)(2,1)S(1)} %get-tuple-element.87, f32[512]{0:T(512)S(1)} %bitcast.488), kind=kOutput, calls=%fused_computation | convolution fusion | flops 538181632 | bytes 2623488 | tf_op jit(solution)/shard_map/dot_general | solution.py:334
  105.2 1.8 convolution_convert_fusion.1
  107.7 18.5 %scatter_dp.3 = (f32[4,32,1024]{2,1,0:T(8,128)}, f32[4,32,1024]{2,1,0:T(8,128)}, f32[4,8,128]{2,1,0:T(8,128)}) custom-call(bf16[2,2,4,32,1024]{4,3,2,1,0:T(8,128)(2,1)} %bitcast.446, bf16[2,2,4,32,1024]{4,3,2,1,0:T(8,128)(2,1)} %bitcast.445, f32[4,8,128]{2,1,0:T(8,128)} %pad.13.aux_ref), custom_call_target="tpu_custom_call" | custom-call | tf_op jit(solution)/shard_map/scatter_dp/pallas_call | solution.py:105
  127.0 1.1 multiply_convert_fusion.2
  128.4 2.1 %select_reduce_fusion.2 = (bf16[16,1024]{1,0:T(8,128)(2,1)S(1)}, bf16[16,1024]{1,0:T(8,128)(2,1)S(1)}, bf16[16,1024]{1,0:T(8,128)(2,1)S(1)}, bf16[16,1024]{1,0:T...) fusion(pred[16,11]{1,0:T(8,128)(4,1)S(1)} %get-tuple-element.73, ...), kind=kLoop, calls=%fused_computation.79 | loop fusion | flops 3506176 | bytes 918032 | tf_op jit(solution)/shard_map/reduce_sum | solution.py:355
  137.3 1.0 copy.149.s_ref
  140.9 21.3 %memory_cell.3 = (f32[16,4,8,256]{3,2,1,0:T(8,128)}, f32[2,16,4,256,256]{4,3,2,1,0:T(8,128)}) custom-call(f32[16,4,8,256]{3,2,1,0:T(8,128)} %maximum_convert_fusion.2.q_ref, f32[16,4,8,256]{3,2,1,0:T(8,128)} %get-tuple-element.34.k_ref, f32[16,4,8,256]{3,2,1,0:T(8,128)} %maximum_convert_fusion.3.v_ref, ...), custom_call_target="tpu_custom_call", output_to_operand_aliasing={{1}: (6, {})} | custom-call | tf_op jit(solution)/shard_map/memory_cell/pallas_call | solution.py:280
  162.2 1.2 reduce_sum.214
  163.5 1.3 multiply_reduce_fusion
  164.8 1.2 multiply_multiply_fusion
  166.1 1.2 fusion.78
  167.3 11.1 %gather_dp.3 = bf16[2,2,4,32,1024]{4,3,2,1,0:T(8,128)(2,1)} custom-call(bf16[4,32,1024]{2,1,0:T(8,128)(2,1)} %bitcast.439), custom_call_target="tpu_custom_call" | custom-call | tf_op jit(solution)/shard_map/gather_dp/pallas_call | solution.py:179
  178.4 3.0 %fusion.3 = bf16[256,512]{1,0:T(8,128)(2,1)} fusion(bf16[512,1024]{1,0:T(8,128)(2,1)} %bitcast.442, bf16[2,1024,512]{2,1,0:T(8,128)(2,1)} %param.34, s32[512]{0:T(512)S(1)} %select_n.124), kind=kOutput, calls=%fused_computation.15 | convolution fusion | flops 537395200 | bytes 2361344 | tf_op jit(solution)/shard_map/dot_general | solution.py:407
  181.4 17.0 %reduce_tp.3 = bf16[4,64,512]{2,1,0:T(8,128)(2,1)} custom-call(bf16[4,64,512]{2,1,0:T(8,128)(2,1)} %bitcast.451, bf16[4,64,512]{2,1,0:T(8,128)(2,1)} %reduce_tp.2.x_ref), custom_call_target="tpu_custom_call" | custom-call | tf_op jit(solution)/shard_map/reduce_tp/pallas_call | solution.py:230
  198.4 2.1 %fusion.29 = bf16[64,8,512]{2,1,0:T(8,128)(2,1)} fusion(bf16[64,8,512]{2,1,0:T(8,128)(2,1)S(1)} %copy-done.8, bf16[256,512]{1,0:T(8,128)(2,1)} %bitcast.449, pred[64,8]{1,0:T(8,128)(4,1)S(1)} %iota_compare_fusion.9, s32[512]{0:T(512)S(1)} %select_n.124), kind=kOutput, calls=%fused_computation.66 | convolution fusion | flops 134873088 | bytes 1313280 | tf_op jit(solution)/shard_map/dot_general | solution.py:409
  (167 shorter events, 21.6 us)
Async XLA Ops:
  0.6 4.0 %copy-start.7 = (bf16[64,8,512]{2,1,0:T(8,128)(2,1)S(1)}, bf16[64,8,512]{2,1,0:T(8,128)(2,1)}, u32[]{:S(2)}) copy-start(bf16[64,8,512]{2,1,0:T(8,128)(2,1)} %param.19) | copy-start | bytes 1572868
  0.6 4.0 %copy-start.21 = (bf16[2,512,1024]{2,1,0:T(8,128)(2,1)S(1)}, bf16[2,512,1024]{2,1,0:T(8,128)(2,1)}, u32[]{:S(2)}) copy-start(bf16[2,512,1024]{2,1,0:T(8,128)(2,1)} %param.23) | copy-start | bytes 6291460
  4.6 1.7 copy-start.18
  6.3 22.4 %copy-start.11 = (bf16[2,16,3,1024]{3,1,2,0:T(8,128)(2,1)S(1)}, bf16[2,16,3,1024]{3,1,2,0:T(8,128)(2,1)}, u32[]{:S(2)}) copy-start(bf16[2,16,3,1024]{3,1,2,0:T(8,128)(2,1)} %param.35) | copy-start | bytes 589828
  7.2 21.8 %copy-start.12 = (f32[2,4,1024]{2,1,0:T(4,128)S(1)}, f32[2,4,1024]{2,1,0:T(4,128)}, u32[]{:S(2)}) copy-start(f32[2,4,1024]{2,1,0:T(4,128)} %param.24) | copy-start | bytes 98308
  28.7 1.2 copy-start.3
  29.0 1.6 copy-start.5
  29.1 2.3 %copy-start.1 = (f32[4,32,1024]{2,1,0:T(8,128)S(1)}, f32[4,32,1024]{2,1,0:T(8,128)}, u32[]{:S(2)}) copy-start(f32[4,32,1024]{2,1,0:T(8,128)} %get-tuple-element.15) | copy-start | bytes 1572868
  29.1 2.4 %copy-start.2 = (bf16[2,4,256,256]{3,2,1,0:T(8,128)(2,1)S(1)}, bf16[2,4,256,256]{3,2,1,0:T(8,128)(2,1)}, u32[]{:S(2)}) copy-start(bf16[2,4,256,256]{3,2,1,0:T(8,128)(2,1)} %param.27) | copy-start | bytes 3145732
  30.0 2.3 %copy-start.14 = (bf16[2,4,768]{2,1,0:T(4,128)(2,1)S(1)}, bf16[2,4,768]{2,1,0:T(4,128)(2,1)}, u32[]{:S(2)}) copy-start(bf16[2,4,768]{2,1,0:T(4,128)(2,1)} %param.28) | copy-start | bytes 36868
  30.3 2.2 %copy-start.15 = (bf16[2,4,768]{2,1,0:T(4,128)(2,1)S(1)}, bf16[2,4,768]{2,1,0:T(4,128)(2,1)}, u32[]{:S(2)}) copy-start(bf16[2,4,768]{2,1,0:T(4,128)(2,1)} %param.29) | copy-start | bytes 36868
  31.4 2.2 %copy-start.19 = (f32[2,4]{1,0:T(2,128)S(1)}, f32[2,4]{1,0:T(2,128)}, u32[]{:S(2)}) copy-start(f32[2,4]{1,0:T(2,128)} %param.30) | copy-start | bytes 100
  31.4 2.2 %copy-start.20 = (f32[2,4]{1,0:T(2,128)S(1)}, f32[2,4]{1,0:T(2,128)}, u32[]{:S(2)}) copy-start(f32[2,4]{1,0:T(2,128)} %param.31) | copy-start | bytes 100
  31.4 2.9 %copy-start.13 = (f32[2,16,4]{1,2,0:T(4,128)S(1)}, f32[2,16,4]{1,2,0:T(4,128)}, u32[]{:S(2)}) copy-start(f32[2,16,4]{1,2,0:T(4,128)} %param.37) | copy-start | bytes 1540
  38.3 24.1 %copy-start.16 = (f32[2,4,256]{2,1,0:T(4,128)S(1)}, f32[2,4,256]{2,1,0:T(4,128)}, u32[]{:S(2)}) copy-start(f32[2,4,256]{2,1,0:T(4,128)} %param.32) | copy-start | bytes 24580
  59.8 3.9 %copy-start.17 = (f32[2,1024]{1,0:T(2,128)S(1)}, f32[2,1024]{1,0:T(2,128)}, u32[]{:S(2)}) copy-start(f32[2,1024]{1,0:T(2,128)} %param.33) | copy-start | bytes 24580
  59.8 3.9 %copy-start.10 = (f32[4,32,1024]{2,1,0:T(8,128)S(1)}, f32[4,32,1024]{2,1,0:T(8,128)}, u32[]{:S(2)}) copy-start(f32[4,32,1024]{2,1,0:T(8,128)} %get-tuple-element.17) | copy-start | bytes 1572868
  64.9 16.2 %copy-start.8 = (bf16[64,8,512]{2,1,0:T(8,128)(2,1)S(1)}, bf16[64,8,512]{2,1,0:T(8,128)(2,1)}, u32[]{:S(2)}) copy-start(bf16[64,8,512]{2,1,0:T(8,128)(2,1)} %param.19) | copy-start | bytes 1572868
  100.6 4.6 %copy-start.22 = (bf16[2,512,1024]{2,1,0:T(8,128)(2,1)S(1)}, bf16[2,512,1024]{2,1,0:T(8,128)(2,1)}, u32[]{:S(2)}) copy-start(bf16[2,512,1024]{2,1,0:T(8,128)(2,1)} %param.22) | copy-start | bytes 6291460
  126.1 5.1 %copy-start = (f32[4,32,1024]{2,1,0:T(8,128)S(1)}, f32[4,32,1024]{2,1,0:T(8,128)}, u32[]{:S(2)}) copy-start(f32[4,32,1024]{2,1,0:T(8,128)} %get-tuple-element.18) | copy-start | bytes 1572868
  131.9 1.2 copy-start.4
  132.0 1.7 copy-start.6
  162.2 3.9 %copy-start.9 = (f32[4,32,1024]{2,1,0:T(8,128)S(1)}, f32[4,32,1024]{2,1,0:T(8,128)}, u32[]{:S(2)}) copy-start(f32[4,32,1024]{2,1,0:T(8,128)} %get-tuple-element.22) | copy-start | bytes 1572868
where the time goes:
time: 203 us; the launch traced here: 201 us
  Pallas kernels  139 us (68%)
  other arithmetic  28.6 us (14%)
  matrix products  24.4 us (12%)
  local copies, waits for them, and re-layouts  7.49 us (4%)
    pallas_call x2, Pallas kernels, memory_cell(): pl.pallas_call(functools.partial(cell_kernel, heads), grid=(batch,), out_...  42.8 us
    pallas_call x2, Pallas kernels, scatter_dp(): pl.pallas_call(functools.partial(scatter_kernel, n, chunks), out_shape=(j...  37.9 us
    pallas_call x2, Pallas kernels, reduce_tp(): pl.pallas_call(functools.partial(reduce_kernel, n), out_shape=jax.ShapeDt...  35.4 us
    pallas_call x2, Pallas kernels, gather_dp(): pl.pallas_call(functools.partial(gather_kernel, n, chunks), out_shape=jax...  23.2 us
    dot_general x2, matrix products, per_device(): part = jnp.dot(packed, w_out[l], preferred_element_type=f32).astype(bf)  5.92 us
    dot_general x2, matrix products, per_device(): first = jnp.dot(scaled, w_branch[l], preferred_element_type=f32).astype(bf)  4.91 us
    dot_general x2, matrix products, per_device(): jnp.dot(scaled, w_silu_gate[l], preferred_element_type=f32).astype(bf)  4.81 us
    dot_general x24, matrix products, project(): jnp.dot(source[:, h * HEAD_DIM:(h + 1) * HEAD_DIM], w[h], preferred_eleme...  4.12 us

commit v1 on v0

--- a/solution.py
+++ b/solution.py
@@ -243,49 +243,179 @@
     return out.reshape(rows, width)
 
 
-def cell_kernel(heads, q_ref, k_ref, v_ref, w_ref, s_ref, c_ref, *rest):
-    num_ref, new_ref = rest[-2:]
+def cell_kernel(layer, model, heads, steps, cnt_ref, bi_ref, bf_ref, br_ref, gt_ref, aux_ref,
+                ccol_ref, crow_ref, mcol_ref, st_ref, cw_ref, wq_ref, wk_ref, wv_ref, wg_ref,
+                og_ref, sg_ref, mem_ref, *rest):
+    (mixed_ref, nc_ref, newmem_ref, nmax_ref,
+     pad_s, conv_s, q_s, k_s, v_s, num_s, car_s, dec_s, cs_s, top_s, nc_s, stage, ins, outs) = rest[-18:]
+    f32 = jnp.float32
+    bf = jnp.bfloat16
+    batch = stage.shape[0]
+    own, width = br_ref.shape
+    dim = HEAD_DIM
+    base = 8 - (CONV - 1)
+
+    def fetch(b):
+        return pltpu.make_async_copy(mem_ref.at[layer, b], stage.at[b], ins.at[b])
+
+    def store(b):
+        return pltpu.make_async_copy(stage.at[b], newmem_ref.at[layer, b], outs.at[b])
+
+    for b in range(batch):
+        fetch(b).start()
+
+    squares = aux_ref[0, 0:1, :own]
+    for i in range(1, aux_ref.shape[0]):
+        squares = squares + aux_ref[i, 0:1, :own]
+    inv_row = lax.rsqrt(squares / model + epsilon)
+    r = lax.broadcasted_iota(jnp.int32, (own, own), 0)
+    c = lax.broadcasted_iota(jnp.int32, (own, own), 1)
+    inv = jnp.sum(jnp.where(r == c, inv_row, 0.0), axis=1, keepdims=True)
+    branch = (br_ref[...] * inv).astype(bf)
+    pad_s[:, 8:8 + steps, :] = branch.astype(f32).reshape(batch, steps, width)
+    for j in range(CONV - 1):
+        rows = st_ref[0, j].astype(f32)
+        for b in range(batch):
+            pad_s[b, base + j:base + j + 1, :] = rows[b:b + 1, :]
+    total = pad_s[:, base:base + steps, :] * cw_ref[0, 0:1, :]
+    for j in range(1, CONV):
+        total = total + pad_s[:, base + j:base + j + steps, :] * cw_ref[0, j:j + 1, :]
+    conv = (total * jax.nn.sigmoid(total)).astype(bf).reshape(own, width)
+    conv_s[...] = conv
+    for b in range(batch):
+        for i in range(CONV - 1):
+            nc_s[i, b:b + 1, :] = pad_s[b, pl.ds(base + i + cnt_ref[b], 1), :]
+    nc_ref[...] = nc_s[...].astype(bf)
+
+    same = (r // steps) == (c // steps)
+    causal = same & (r >= c)
+    behind = same & (r <= c)
+    live_col = (r[:, 0:1] % steps) < ccol_ref[...]
+    live_row = (c[0:1, :] % steps) < crow_ref[...]
+    nt = (((1,), (1,)), ((), ()))
     for h in range(heads):
-        q = q_ref[0, h]
-        k = k_ref[0, h]
-        v = v_ref[0, h]
-        scal = s_ref[0, h]
-        old = c_ref[0, 0, h]
-        scores = lax.dot_general(q, k, (((1,), (1,)), ((), ())), preferred_element_type=jnp.float32)
-        scores = scores * w_ref[0, h]
-        inside = jnp.dot(scores, v, preferred_element_type=jnp.float32)
-        carried = jnp.dot(
-            q.astype(jnp.bfloat16), old.astype(jnp.bfloat16), preferred_element_type=jnp.float32
-        )
-        num_ref[0, h] = inside + scal[:, 0:1] * carried
-        outer = lax.dot_general(
-            k * scal[:, 1:2], v, (((0,), (0,)), ((), ())), preferred_element_type=jnp.float32
-        )
-        new_ref[0, 0, h] = scal[0:1, 2:3] * old + outer
-
-
-def memory_cell(layer, q, k, v, weights, scal, memory, previous):
-    batch, heads, steps, dim = q.shape
-    row = pl.BlockSpec((1, heads, steps, dim), lambda b: (b, 0, 0, 0))
-    small = pl.BlockSpec((1, heads, steps, steps), lambda b: (b, 0, 0, 0))
-    three = pl.BlockSpec((1, heads, steps, 3), lambda b: (b, 0, 0, 0))
-    mat = pl.BlockSpec((1, 1, heads, dim, dim), lambda b: (layer, b, 0, 0, 0))
-    args = [q, k, v, weights, scal, memory]
-    specs = [row, row, row, small, three, mat]
+        sl = slice(h * dim, (h + 1) * dim)
+        q = jnp.dot(conv[:, sl], wq_ref[0, h], preferred_element_type=f32).astype(bf)
+        k = jnp.dot(conv[:, sl], wk_ref[0, h], preferred_element_type=f32).astype(bf)
+        v = jnp.dot(branch[:, sl], wv_ref[0, h], preferred_element_type=f32).astype(bf)
+        gcol = None
+        for i, part in enumerate((q, k, v)):
+            w = wg_ref[0, h, :, i * dim:(i + 1) * dim]
+            one = lax.dot_general(part, w, nt, preferred_element_type=f32)
+            two = lax.dot_general(w, part, nt, preferred_element_type=f32)
+            gcol, grow = (one, two) if gcol is None else (gcol + one, grow + two)
+        bias_i = bi_ref[layer, h]
+        bias_f = bf_ref[layer, h]
+
+        def log_sig(x):
+            return jnp.minimum(x, 0.0) - jnp.log1p(jnp.exp(-jnp.abs(x)))
+
+        ig_col = jnp.where(live_col, gcol[:, 0:1] + bias_i, very_negative)
+        ig_row = jnp.where(live_row, grow[0:1, :] + bias_i, very_negative)
+        fg_col = jnp.where(live_col, log_sig(gcol[:, 1:2] + bias_f), 0.0)
+        fg_row = jnp.where(live_row, log_sig(grow[1:2, :] + bias_f), 0.0)
+        cum_col = jnp.sum(jnp.where(causal, fg_row, 0.0), axis=1, keepdims=True)
+        end_col = jnp.sum(jnp.where(same, fg_row, 0.0), axis=1, keepdims=True)
+        cum_row = jnp.sum(jnp.where(behind, fg_col, 0.0), axis=0, keepdims=True)
+        lift_row = ig_row - cum_row
+        logw = jnp.where(causal, cum_col + lift_row, very_negative)
+        old_max = mcol_ref[:, h:h + 1]
+        carried = cum_col + old_max
+        stab = jnp.maximum(jnp.max(logw, axis=1, keepdims=True), carried)
+        weights = jnp.exp(logw - stab)
+        top = jnp.max(jnp.where(same, end_col + lift_row, very_negative), axis=1, keepdims=True)
+        new_max = jnp.maximum(top, end_col + old_max)
+        update = jnp.exp(end_col - cum_col + ig_col - new_max)
+        top_s[:, h:h + 1] = new_max
+        dec_s[:, h:h + 1] = jnp.exp(end_col + old_max - new_max)
+        cs_s[:, h:h + 1] = jnp.exp(carried - stab)
+        scores = lax.dot_general(q, k, nt, preferred_element_type=f32)
+        scores = (jnp.where(causal, scores, 0.0) * (dim ** -0.5) * weights).astype(bf)
+        num_s[:, sl] = jnp.dot(scores, v, preferred_element_type=f32)
+        q_s[:, sl] = q.astype(f32)
+        k_s[:, sl] = k.astype(f32) * (dim ** -0.5) * update
+        v_s[:, sl] = v.astype(f32)
+    nmax_ref[...] = top_s[pl.ds(steps - 1, batch, stride=steps), :]
+
+    @pl.loop(0, batch)
+    def _(b):
+        fetch(b).wait()
+        rows = pl.ds(pl.multiple_of(b * steps, 8), steps)
+        for h in range(heads):
+            sl = slice(h * dim, (h + 1) * dim)
+            old = stage[b, h]
+            car_s[rows, sl] = jnp.dot(q_s[rows, sl].astype(bf), old.astype(bf), preferred_element_type=f32)
+            outer = lax.dot_general(
+                k_s[rows, sl].astype(bf), v_s[rows, sl].astype(bf), (((0,), (0,)), ((), ())),
+                preferred_element_type=f32,
+            )
+            stage[b, h] = dec_s[rows, :][0:1, h:h + 1] * old + outer
+        store(b).start()
+
+    live = (lax.broadcasted_iota(jnp.int32, (own, 1), 0) % steps) < ccol_ref[...]
+    for h in range(heads):
+        sl = slice(h * dim, (h + 1) * dim)
+        num = num_s[:, sl] + cs_s[:, h:h + 1] * car_s[:, sl]
+        centered = num - jnp.mean(num, axis=1, keepdims=True)
+        normal = centered * lax.rsqrt(jnp.mean(centered * centered, axis=1, keepdims=True) + epsilon)
+        gate = (gt_ref[:, sl] * inv).astype(bf).astype(f32)
+        mixed = normal * og_ref[0, h:h + 1, :] + sg_ref[layer:layer + 1, sl] * conv_s[:, sl].astype(f32)
+        mixed = mixed * (gate * jax.nn.sigmoid(gate))
+        mixed_ref[:, sl] = jnp.where(live, mixed, 0.0).astype(bf)
+    for b in range(batch):
+        store(b).wait()
+
+
+def memory_cell(layer, model, steps, counts, bias_input, bias_forget, branch, gate, aux, count_col,
+                count_row, old_max, state, conv_weight, w_query, w_key, w_value, w_gates, out_gain,
+                skip_gain, memory, previous):
+    _, batch, heads, dim, _ = memory.shape
+    own, width = branch.shape
+    f32 = jnp.float32
+
+    def whole(a):
+        return pl.BlockSpec(a.shape, lambda i: (0,) * a.ndim)
+
+    def layered(a):
+        return pl.BlockSpec((1,) + a.shape[1:], lambda i: (layer,) + (0,) * (a.ndim - 1))
+
+    smem = pl.BlockSpec(memory_space=pltpu.SMEM)
+    anyspace = pl.BlockSpec(memory_space=pl.ANY)
+    args = [counts, bias_input, bias_forget, branch, gate, aux, count_col, count_row, old_max,
+            state, conv_weight, w_query, w_key, w_value, w_gates, out_gain, skip_gain, memory]
+    specs = [smem, smem, smem] + [whole(a) for a in args[3:9]] + [layered(a) for a in args[9:16]]
+    specs += [whole(skip_gain), anyspace]
     aliases = {}
     if previous is not None:
+        aliases = {len(args): 2}
         args.append(previous)
-        specs.append(pl.BlockSpec(memory_space=pl.ANY))
-        aliases = {6: 1}
+        specs.append(anyspace)
+    big = pltpu.VMEM((own, width), f32)
+    small = pltpu.VMEM((own, 128), f32)
     return pl.pallas_call(
-        functools.partial(cell_kernel, heads),
-        grid=(batch,),
+        functools.partial(cell_kernel, layer, model, heads, steps),
+        grid=(1,),
         out_shape=(
-            jax.ShapeDtypeStruct(q.shape, jnp.float32),
-            jax.ShapeDtypeStruct(memory.shape, jnp.float32),
+            jax.ShapeDtypeStruct((own, width), jnp.bfloat16),
+            jax.ShapeDtypeStruct((CONV - 1, batch, width), jnp.bfloat16),
+            jax.ShapeDtypeStruct(memory.shape, f32),
+            jax.ShapeDtypeStruct((batch, 128), f32),
         ),
         in_specs=specs,
-        out_specs=(row, mat),
+        out_specs=(
+            pl.BlockSpec((own, width), lambda i: (0, 0)),
+            pl.BlockSpec((CONV - 1, batch, width), lambda i: (0, 0, 0)),
+            anyspace,
+            pl.BlockSpec((batch, 128), lambda i: (0, 0)),
+        ),
+        scratch_shapes=[
+            pltpu.VMEM((batch, 8 + steps, width), f32),
+            pltpu.VMEM((own, width), jnp.bfloat16),
+            big, big, big, big, big, small, small, small,
+            pltpu.VMEM((CONV - 1, batch, width), f32),
+            pltpu.VMEM((batch, heads, dim, dim), f32),
+            pltpu.SemaphoreType.DMA((batch,)), pltpu.SemaphoreType.DMA((batch,)),
+        ],
         input_output_aliases=aliases,
         compiler_params=pltpu.CompilerParams(dimension_semantics=("arbitrary",)),
         name="memory_cell",
@@ -310,11 +440,13 @@
     model = features * ndp
     flat_tokens = tokens.reshape(rows, features)
     positions = jnp.arange(steps, dtype=jnp.int32)
-    live = positions[None, :] < live_counts[:, None]
-    causal = positions[:, None] >= positions[None, :]
-    picks = live_counts[:, None] + jnp.arange(CONV - 1, dtype=jnp.int32)[None, :]
-    pick_hot = picks[:, :, None] == jnp.arange(steps + CONV - 1, dtype=jnp.int32)[None, None, :]
     count_row = jnp.pad(live_counts.astype(f32), (0, lanes - batch))
+
+    count_col = jnp.repeat(live_counts, steps)[:, None]
+    count_lane = jnp.repeat(live_counts, steps)[None, :]
+    old_max = jnp.repeat(max_state, steps, axis=1)
+    states = jnp.transpose(conv_state, (0, 2, 1, 3))
+    w_gates = jnp.pad(jnp.stack([w_input_gate, w_forget_gate], axis=2), ((0, 0), (0, 0), (0, 6), (0, 0)))
 
     dense = flat_tokens
     compact = None
@@ -333,10 +465,6 @@
         first = jnp.dot(scaled, w_branch[l], preferred_element_type=f32).astype(bf)
         second = jnp.dot(scaled, w_silu_gate[l], preferred_element_type=f32).astype(bf)
         branch, gate, aux = scatter_dp(ndp, first, second, aux)
-        total = jnp.sum(aux[:, 0, :own], axis=0)
-        inv = lax.rsqrt(total / model + epsilon)[:, None]
-        branch = (branch * inv).astype(bf).reshape(batch, steps, width)
-        gate = (gate * inv).astype(bf).astype(f32).reshape(batch, steps, width)
         if select is None:
             counts = aux[:, 1, :batch].astype(jnp.int32).reshape(all_batch)
             ids = jnp.arange(all_batch)
@@ -346,62 +474,13 @@
             select = (jnp.arange(live_rows)[:, None] == place[None, :]).astype(bf)
             compact = jnp.dot(select, flat_tokens, preferred_element_type=f32).astype(bf)
 
-        padded = jnp.concatenate([conv_state[l], branch], axis=1).astype(f32)
-        conv_sum = padded[:, 0:steps] * conv_weight[l, 0]
-        for j in range(1, CONV):
-            conv_sum = conv_sum + padded[:, j:j + steps] * conv_weight[l, j]
-        convolved = jax.nn.silu(conv_sum).astype(bf)
-        new_conv = jnp.stack(
-            [jnp.sum(jnp.where(pick_hot[:, i, :, None], padded, 0.0), axis=1) for i in range(CONV - 1)],
-            axis=1,
-        ).astype(bf)
+        mixed, new_conv, new_memory, new_max = memory_cell(
+            l, model, steps, live_counts, bias_input, bias_forget, branch, gate, aux, count_col,
+            count_lane, old_max[l], states, conv_weight, w_query, w_key, w_value, w_gates,
+            out_gain, skip_gain, memory, new_memory
+        )
         conv_list.append(new_conv)
-        conv_flat = convolved.reshape(own, width)
-        branch_flat = branch.reshape(own, width)
-
-        def project(source, w):
-            parts = [
-                jnp.dot(source[:, h * HEAD_DIM:(h + 1) * HEAD_DIM], w[h], preferred_element_type=f32)
-                for h in range(heads)
-            ]
-            out = jnp.stack([p.reshape(batch, steps, HEAD_DIM) for p in parts], axis=1)
-            return out.astype(bf).astype(f32)
-
-        q = project(conv_flat, w_query[l])
-        k = project(conv_flat, w_key[l])
-        v = project(branch_flat, w_value[l])
-
-        def gate_dot(w, bias):
-            w = w.astype(f32).reshape(heads, 3, 1, HEAD_DIM)
-            return jnp.sum(q * w[:, 0] + k * w[:, 1] + v * w[:, 2], axis=-1) + bias[:, None]
-
-        live_h = live[:, None, :]
-        ig = jnp.where(live_h, gate_dot(w_input_gate[l], bias_input[l]), very_negative)
-        fg = jnp.where(live_h, jax.nn.log_sigmoid(gate_dot(w_forget_gate[l], bias_forget[l])), 0.0)
-        cum = jnp.sum(jnp.where(causal, fg[..., None, :], 0.0), axis=-1)
-        logw = cum[..., :, None] - cum[..., None, :] + ig[..., None, :]
-        logw = jnp.where(causal, logw, very_negative)
-        carried = cum + max_state[l][..., None]
-        stab = jnp.maximum(jnp.max(logw, axis=-1), carried)
-        weights = jnp.exp(logw - stab[..., None])
-        new_max = stab[..., -1]
-        decay = jnp.exp(cum[..., -1] + max_state[l] - new_max)
-        upd = jnp.exp(cum[..., -1:] - cum + ig - new_max[..., None])
-        scal = jnp.stack(
-            [jnp.exp(carried - stab), upd, jnp.broadcast_to(decay[..., None], upd.shape)], axis=-1
-        )
-        max_list.append(new_max)
-        num, new_memory = memory_cell(
-            l, q, k * HEAD_DIM ** (-0.5), v, weights, scal, memory, new_memory
-        )
-        centered = num - jnp.mean(num, axis=-1, keepdims=True)
-        normalized = centered * lax.rsqrt(
-            jnp.mean(centered * centered, axis=-1, keepdims=True) + epsilon
-        )
-        normalized = normalized * out_gain[l][None, :, None, :]
-        readout = jnp.transpose(normalized, (0, 2, 1, 3)).reshape(batch, steps, width)
-        mixed = (readout + skip_gain[l] * convolved.astype(f32)) * jax.nn.silu(gate)
-        mixed = jnp.where(live[:, :, None], mixed, 0.0).astype(bf).reshape(own, width)
+        max_list.append(new_max[:, :heads])
         everyone = gather_dp(ndp, mixed)
         packed = jnp.dot(select, everyone, preferred_element_type=f32).astype(bf)
         part = jnp.dot(packed, w_out[l], preferred_element_type=f32).astype(bf)
@@ -410,7 +489,7 @@
             select, compact, (((0,), (0,)), ((), ())), preferred_element_type=f32
         ).astype(bf)
     result = jnp.where(live_all[:, :, None], dense.reshape(tokens.shape), tokens)
-    return (result, jnp.stack(conv_list), new_memory, jnp.stack(max_list))
+    return (result, jnp.transpose(jnp.stack(conv_list), (0, 2, 1, 3)), new_memory, jnp.stack(max_list))
 
 
 def solution(mesh):

time: 203 us -> 160 us (0.79)
  other arithmetic: 28.6 us -> 4.11 us
  Pallas kernels: 139 us -> 130 us
  matrix products: 24.4 us -> 18.9 us
    reduce_sum x13 -> x0, other arithmetic: 11.6 us -> none  [the longest x2 2.62 us: per_device(): jnp.mean(centered * centered, axis=-1, keepdims=True) + epsilon]
    pallas_call x2, Pallas kernels: 42.8 us -> 33.4 us  [memory_cell(): pl.pallas_call(functools.partial(cell_kernel, layer, model, heads, steps)...]
    convert_element_type x15 -> x0, other arithmetic: 8 us -> none  [the longest x3 2.74 us: project(): return out.astype(bf).astype(f32)]
    dot_general x24 -> x0, matrix products: 4.12 us -> none  [project(): jnp.dot(source[:, h * HEAD_DIM:(h + 1) * HEAD_DIM], w[h], preferred_eleme...]
    mul x2 -> x0, other arithmetic: 2.49 us -> none  [per_device(): normalized = normalized * out_gain[l][None, :, None, :]]
    exp x6 -> x0, other arithmetic: 2.05 us -> none  [the longest x2 1.85 us: per_device(): weights = jnp.exp(logw - stab[..., None])]
where the time goes in v1:
time: 160 us
  Pallas kernels  130 us (81%)
  matrix products  18.9 us (12%)
  local copies, waits for them, and re-layouts  6.09 us (4%)
  other arithmetic  4.11 us (3%)
    pallas_call x2, Pallas kernels, scatter_dp(): pl.pallas_call(functools.partial(scatter_kernel, n, chunks), out_shape=(j...  37.9 us
    pallas_call x2, Pallas kernels, reduce_tp(): pl.pallas_call(functools.partial(reduce_kernel, n), out_shape=jax.ShapeDt...  35.5 us
    pallas_call x2, Pallas kernels, memory_cell(): pl.pallas_call(functools.partial(cell_kernel, layer, model, heads, steps)...  33.4 us
    pallas_call x2, Pallas kernels, gather_dp(): pl.pallas_call(functools.partial(gather_kernel, n, chunks), out_shape=jax...  23.1 us
    dot_general x2, matrix products, per_device(): part = jnp.dot(packed, w_out[l], preferred_element_type=f32).astype(bf)  5.92 us
    dot_general x2, matrix products, per_device(): first = jnp.dot(scaled, w_branch[l], preferred_element_type=f32).astype(bf)  4.86 us
    dot_general x2, matrix products, per_device(): lax.dot_general(select, compact, (((0,), (0,)), ((), ())), preferred_elem...  3.59 us
    dot_general x2, matrix products, per_device(): jnp.dot(scaled, w_silu_gate[l], preferred_element_type=f32).astype(bf)  3.52 us

profile of v1, /device:TPU:0, one launch (start us, length us, event | category | flops | bytes accessed | tf_op | source)
XLA Modules:
  0.0 159.8 jit_solution(14247335040930185903)
XLA Ops:
  0.7 0.9 fusion.38
  1.5 3.1 %convolution_convert_fusion.3 = bf16[512,1024]{1,0:T(8,128)(2,1)} fusion(bf16[2,512,1024]{2,1,0:T(8,128)(2,1)} %param.22, bf16[64,8,512]{2,1,0:T(8,128)(2,1)} %param.19, f32[512]{0:T(512)S(1)} %bitcast.104), kind=kOutput, calls=%fused_computation.3 | convolution fusion | flops 538181632 | bytes 2623488 | tf_op jit(solution)/shard_map/dot_general | solution.py:465
  4.6 1.7 %convolution_convert_fusion.2 = bf16[512,1024]{1,0:T(8,128)(2,1)} fusion(bf16[2,512,1024]{2,1,0:T(8,128)(2,1)S(1)} %copy-done.7, bf16[64,8,512]{2,1,0:T(8,128)(2,1)S(1)} %copy-done, f32[512]{0:T(512)S(1)} %bitcast.105), kind=kOutput, calls=%fused_computation.2 | convolution fusion | flops 538181632 | bytes 2623488 | tf_op jit(solution)/shard_map/dot_general | solution.py:466
  6.3 0.2 fusion.7
  6.6 0.6 pad.16.aux_ref
  7.2 19.4 %scatter_dp.2 = (f32[4,32,1024]{2,1,0:T(8,128)}, f32[4,32,1024]{2,1,0:T(8,128)}, f32[4,8,128]{2,1,0:T(8,128)}) custom-call(bf16[2,2,4,32,1024]{4,3,2,1,0:T(8,128)(2,1)} %bitcast.76, bf16[2,2,4,32,1024]{4,3,2,1,0:T(8,128)(2,1)} %bitcast.77, f32[4,8,128]{2,1,0:T(8,128)} %pad.16.aux_ref), custom_call_target="tpu_custom_call" | custom-call | tf_op jit(solution)/shard_map/scatter_dp/pallas_call | solution.py:105
  26.7 0.7 broadcast_in_dim_reshape.11.ccol_ref
  27.4 0.6 broadcast_in_dim_reshape.10.crow_ref
  28.1 0.7 fusion.37.wg_ref
  28.9 0.6 broadcast_bitcast_fusion.1.mcol_ref
  29.5 16.3 %memory_cell.2 = (bf16[128,1024]{1,0:T(8,128)(2,1)}, bf16[3,16,1024]{2,1,0:T(8,128)(2,1)}, f32[2,16,4,256,256]{4,3,2,1,0:T(8,128)}, f32[16,128]{1,0:T(8,128)}) custom-call(s32[16]{0:T(128)} %cnt_ref.3, f32[2,4]{1,0:T(2,128)} %bi_ref.3, f32[2,4]{1,0:T(2,128)} %bf_ref.3, f32[128,1024]{1,0:T(8,128)} %bitcast.82, f32[128,1024]{1,0:T(8,128)} %bitcast.83, ...), custom_call_target="tpu_custom_call" | custom-call | tf_op jit(solution)/shard_map/memory_cell/pallas_call | solution.py:395
  45.8 12.0 %gather_dp.2 = bf16[2,2,4,32,1024]{4,3,2,1,0:T(8,128)(2,1)} custom-call(bf16[4,32,1024]{2,1,0:T(8,128)(2,1)} %bitcast.87), custom_call_target="tpu_custom_call" | custom-call | tf_op jit(solution)/shard_map/gather_dp/pallas_call | solution.py:179
  57.9 0.7 convert_reduce_fusion
  58.7 0.1 select_reduce_fusion
  58.8 0.1 add_select_fusion
  59.0 3.0 %fusion.4 = bf16[256,512]{1,0:T(8,128)(2,1)} fusion(bf16[512,1024]{1,0:T(8,128)(2,1)} %bitcast.74, bf16[2,1024,512]{2,1,0:T(8,128)(2,1)} %param.34, s32[512]{0:T(512)S(1)} %select_n.21), kind=kOutput, calls=%fused_computation.16 | convolution fusion | flops 537395200 | bytes 2361344 | tf_op jit(solution)/shard_map/dot_general | solution.py:486
  62.0 1.0 convolution_convert_fusion.8
  63.0 18.5 %reduce_tp.2.x_ref = bf16[4,64,512]{2,1,0:T(8,128)(2,1)} custom-call(bf16[4,64,512]{2,1,0:T(8,128)(2,1)} %bitcast.89, bf16[4,64,512]{2,1,0:T(8,128)(2,1)} %bitcast.91), custom_call_target="tpu_custom_call" | custom-call | tf_op jit(solution)/shard_map/reduce_tp/pallas_call | solution.py:230
  81.4 1.5 fusion.9
  82.9 1.8 %convolution_convert_fusion = bf16[512,1024]{1,0:T(8,128)(2,1)} fusion(bf16[2,512,1024]{2,1,0:T(8,128)(2,1)S(1)} %copy-done.7, bf16[512,512]{0,1:T(8,128)(2,1)S(1)} %get-tuple-element.37, f32[512]{0:T(512)S(1)} %bitcast.101), kind=kOutput, calls=%fused_computation | convolution fusion | flops 538181632 | bytes 2623488 | tf_op jit(solution)/shard_map/dot_general | solution.py:466
  84.8 1.8 %convolution_convert_fusion.1 = bf16[512,1024]{1,0:T(8,128)(2,1)} fusion(bf16[2,512,1024]{2,1,0:T(8,128)(2,1)S(1)} %copy-done.8, bf16[512,512]{0,1:T(8,128)(2,1)S(1)} %get-tuple-element.37, f32[512]{0:T(512)S(1)} %bitcast.102), kind=kOutput, calls=%fused_computation.1 | convolution fusion | flops 538181632 | bytes 2623488 | tf_op jit(solution)/shard_map/dot_general | solution.py:465
  86.6 0.6 pad.18.aux_ref
  87.2 18.5 %scatter_dp.3 = (f32[4,32,1024]{2,1,0:T(8,128)}, f32[4,32,1024]{2,1,0:T(8,128)}, f32[4,8,128]{2,1,0:T(8,128)}) custom-call(bf16[2,2,4,32,1024]{4,3,2,1,0:T(8,128)(2,1)} %bitcast.79, bf16[2,2,4,32,1024]{4,3,2,1,0:T(8,128)(2,1)} %bitcast.78, f32[4,8,128]{2,1,0:T(8,128)} %pad.18.aux_ref), custom_call_target="tpu_custom_call" | custom-call | tf_op jit(solution)/shard_map/scatter_dp/pallas_call | solution.py:105
  105.7 0.6 broadcast_bitcast_fusion.mcol_ref
  106.4 17.1 %memory_cell.3 = (bf16[128,1024]{1,0:T(8,128)(2,1)}, bf16[3,16,1024]{2,1,0:T(8,128)(2,1)}, f32[2,16,4,256,256]{4,3,2,1,0:T(8,128)}, f32[16,128]{1,0:T(8,128)}) custom-call(s32[16]{0:T(128)} %cnt_ref.3, f32[2,4]{1,0:T(2,128)} %bi_ref.3, f32[2,4]{1,0:T(2,128)} %bf_ref.3, f32[128,1024]{1,0:T(8,128)} %bitcast.84, ...), custom_call_target="tpu_custom_call", output_to_operand_aliasing={{2}: (18, {})} | custom-call | tf_op jit(solution)/shard_map/memory_cell/pallas_call | solution.py:395
  123.5 0.8 copy.47
  124.4 0.6 pad_maximum_fusion.2
  125.0 1.6 maximum_bitcast_fusion
  126.6 11.1 %gather_dp.3 = bf16[2,2,4,32,1024]{4,3,2,1,0:T(8,128)(2,1)} custom-call(bf16[4,32,1024]{2,1,0:T(8,128)(2,1)} %bitcast.86), custom_call_target="tpu_custom_call" | custom-call | tf_op jit(solution)/shard_map/gather_dp/pallas_call | solution.py:179
  137.7 3.0 %fusion.3 = bf16[256,512]{1,0:T(8,128)(2,1)} fusion(bf16[512,1024]{1,0:T(8,128)(2,1)} %bitcast.75, bf16[2,1024,512]{2,1,0:T(8,128)(2,1)} %param.34, s32[512]{0:T(512)S(1)} %select_n.21), kind=kOutput, calls=%fused_computation.15 | convolution fusion | flops 537395200 | bytes 2361344 | tf_op jit(solution)/shard_map/dot_general | solution.py:486
  140.6 17.0 %reduce_tp.3 = bf16[4,64,512]{2,1,0:T(8,128)(2,1)} custom-call(bf16[4,64,512]{2,1,0:T(8,128)(2,1)} %bitcast.90, bf16[4,64,512]{2,1,0:T(8,128)(2,1)} %reduce_tp.2.x_ref), custom_call_target="tpu_custom_call" | custom-call | tf_op jit(solution)/shard_map/reduce_tp/pallas_call | solution.py:230
  157.7 2.1 %fusion.5 = bf16[64,8,512]{2,1,0:T(8,128)(2,1)} fusion(bf16[64,8,512]{2,1,0:T(8,128)(2,1)S(1)} %copy-done, bf16[256,512]{1,0:T(8,128)(2,1)} %bitcast.88, pred[64,8]{1,0:T(8,128)(4,1)S(1)} %iota_compare_fusion.10, s32[512]{0:T(512)S(1)} %select_n.21), kind=kOutput, calls=%fused_computation.18 | convolution fusion | flops 134873088 | bytes 1313280 | tf_op jit(solution)/shard_map/dot_general | solution.py:488
  (34 shorter events, 0.8 us)
Async XLA Ops:
  0.6 4.0 %copy-start = (bf16[64,8,512]{2,1,0:T(8,128)(2,1)S(1)}, bf16[64,8,512]{2,1,0:T(8,128)(2,1)}, u32[]{:S(2)}) copy-start(bf16[64,8,512]{2,1,0:T(8,128)(2,1)} %param.19) | copy-start | bytes 1572868
  0.6 4.0 %copy-start.7 = (bf16[2,512,1024]{2,1,0:T(8,128)(2,1)S(1)}, bf16[2,512,1024]{2,1,0:T(8,128)(2,1)}, u32[]{:S(2)}) copy-start(bf16[2,512,1024]{2,1,0:T(8,128)(2,1)} %param.23) | copy-start | bytes 6291460
  4.6 1.7 %copy-start.5 = (s32[16]{0:T(128)S(1)}, s32[16]{0:T(128)}, u32[]{:S(2)}) copy-start(s32[16]{0:T(128)} %cnt_ref.3) | copy-start | bytes 196
  6.3 21.8 %copy-start.2 = (bf16[2,4,768]{2,1,0:T(4,128)(2,1)S(1)}, bf16[2,4,768]{2,1,0:T(4,128)(2,1)}, u32[]{:S(2)}) copy-start(bf16[2,4,768]{2,1,0:T(4,128)(2,1)} %param.28) | copy-start | bytes 36868
  6.3 21.8 %copy-start.3 = (bf16[2,4,768]{2,1,0:T(4,128)(2,1)S(1)}, bf16[2,4,768]{2,1,0:T(4,128)(2,1)}, u32[]{:S(2)}) copy-start(bf16[2,4,768]{2,1,0:T(4,128)(2,1)} %param.29) | copy-start | bytes 36868
  6.3 22.5 %copy-start.6 = (f32[2,16,4]{1,2,0:T(4,128)S(1)}, f32[2,16,4]{1,2,0:T(4,128)}, u32[]{:S(2)}) copy-start(f32[2,16,4]{1,2,0:T(4,128)} %param.37) | copy-start | bytes 1540
  81.4 3.3 %copy-start.8 = (bf16[2,512,1024]{2,1,0:T(8,128)(2,1)S(1)}, bf16[2,512,1024]{2,1,0:T(8,128)(2,1)}, u32[]{:S(2)}) copy-start(bf16[2,512,1024]{2,1,0:T(8,128)(2,1)} %param.22) | copy-start | bytes 6291460
  106.4 17.9 %copy-start.4 = (f32[16,128]{1,0:T(8,128)S(1)}, f32[16,128]{1,0:T(8,128)}, u32[]{:S(2)}) copy-start(f32[16,128]{1,0:T(8,128)} %get-tuple-element.30) | copy-start | bytes 24580
  106.4 18.6 %copy-start.1 = (bf16[3,16,1024]{2,1,0:T(8,128)(2,1)S(1)}, bf16[3,16,1024]{2,1,0:T(8,128)(2,1)}, u32[]{:S(2)}) copy-start(bf16[3,16,1024]{2,1,0:T(8,128)(2,1)} %get-tuple-element.27) | copy-start | bytes 294916

commit v2 on v1

v2 whole, which is shorter than its diff:
```python
import functools

import jax
import jax.numpy as jnp
from jax import lax
from jax.experimental import pallas as pl
from jax.experimental.pallas import tpu as pltpu
from jax.sharding import PartitionSpec as P

HEAD_DIM = 256
CONV = 4
LAYERS = 2
epsilon = 1e-06
very_negative = -1e30

VM = pl.BlockSpec(memory_space=pltpu.VMEM)
MESH = pl.DeviceIdType.MESH


def rcopy(src, dst, send, recv, axis, device):
    return pltpu.make_async_remote_copy(
        src_ref=src, dst_ref=dst, send_sem=send, recv_sem=recv,
        device_id={axis: device}, device_id_type=MESH,
    )


def bridge_kernel(ndp, ntp, steps, do_out, do_in, dense_res, lo, li, names, *refs):
    R = dict(zip(names, refs))
    f32 = jnp.float32
    bf = jnp.bfloat16
    nx = ndp // 2
    me = lax.axis_index("dp")
    core = me % 2
    x = me // 2
    partner = me + 1 - 2 * core
    z = lax.axis_index("tp")
    loads = []
    for name, layer in (("wo", lo), ("wb", li), ("wg", li)):
        if name in R:
            cp = pltpu.make_async_copy(R[name].at[layer], R[name + "_s"], R[name + "_m"])
            cp.start()
            loads.append(cp)
    barrier = pltpu.get_barrier_semaphore()
    for off in range(1, ndp):
        pl.semaphore_signal(barrier, inc=1, device_id={"dp": (me + off) % ndp}, device_id_type=MESH)
    greeted = ndp - 1
    if do_out and ntp > 1:
        @pl.when(z > 0)
        def _():
            pl.semaphore_signal(barrier, inc=1, device_id={"tp": z - 1}, device_id_type=MESH)

        @pl.when(z < ntp - 1)
        def _():
            pl.semaphore_signal(barrier, inc=1, device_id={"tp": z + 1}, device_id_type=MESH)
        greeted = greeted + jnp.where(z > 0, 1, 0) + jnp.where(z < ntp - 1, 1, 0)
    sent = []

    def start(cp):
        cp.start()
        sent.append(cp)
        return cp

    if do_out:
        m_ref, got, acc_s, sel_s, auxin = R["m"], R["got"], R["acc"], R["sel"], R["auxin"]
        chunks, piece, width = got.shape[2:]
        own = chunks * piece
        live_rows, feats = acc_s.shape
        pl.semaphore_wait(barrier, greeted)
        across = {}
        for c in range(chunks):
            for g in range(nx - 1):
                to = 2 * ((x + 1 + g) % nx) + core
                across[g, c] = start(rcopy(m_ref.at[c], got.at[x, core, c], R["ga_s"].at[g, c],
                                           R["ga_r"].at[g, c], "dp", to))
        near = start(rcopy(m_ref, got.at[x, core], R["gp_s"], R["gp_r"], "dp", partner))

        r = lax.broadcasted_iota(jnp.int32, (own, own), 0)
        c = lax.broadcasted_iota(jnp.int32, (own, own), 1)
        upper = jnp.where(r < c, 1.0, 0.0).astype(bf)
        slot = (c[0:1, :] % steps).astype(f32)
        target = lax.broadcasted_iota(jnp.int32, (live_rows, own), 0).astype(f32)
        offset = jnp.zeros((1, 1), f32)
        for d in range(ndp):
            live = jnp.where(slot < auxin[d, 1:2, :own], 1.0, 0.0)
            ahead = jnp.dot(jnp.broadcast_to(live, (8, own)).astype(bf), upper,
                            preferred_element_type=f32)[0:1, :]
            place = jnp.where(live > 0.5, ahead + offset, -1.0)
            offset = offset + jnp.sum(live, axis=1, keepdims=True)
            sel_s[d] = jnp.where(target == place, 1.0, 0.0).astype(bf)
        loads[0].wait()
        wo = R["wo_s"]

        def packed(d, rows):
            part = jnp.dot(rows, wo[...], preferred_element_type=f32).astype(bf)
            return jnp.dot(sel_s[d], part, preferred_element_type=f32)

        acc_s[...] = packed(me, m_ref[...].reshape(own, width))
        if dense_res:
            total = jnp.dot(sel_s[0], R["tok"][0], preferred_element_type=f32)
            for d in range(1, ndp):
                total = total + jnp.dot(sel_s[d], R["tok"][d], preferred_element_type=f32)
            R["res_s"][...] = total.astype(bf)
            res = R["res_s"]
        else:
            res = R["res"]
        near.wait_recv()
        acc_s[...] += packed(partner, got[x, 1 - core].reshape(own, width))
        passed = []
        for c in range(chunks):
            for g in range(nx - 1):
                origin = (x + nx - 1 - g) % nx
                across[g, c].wait_recv()
                spot = got.at[origin, core, c]
                passed.append(start(rcopy(spot, spot, R["gf_s"].at[g, c], R["gf_r"].at[g, c],
                                          "dp", partner)))
        for g in range(nx - 1):
            origin = (x + nx - 1 - g) % nx
            acc_s[...] += packed(2 * origin + core, got[origin, core].reshape(own, width))
        for cp in passed:
            cp.wait_recv()
        for g in range(nx - 1):
            origin = (x + nx - 1 - g) % nx
            acc_s[...] += packed(2 * origin + 1 - core, got[origin, 1 - core].reshape(own, width))

        xo = R["xo"]
        kz, rz = xo.shape[:2]
        half = ntp // 2
        zsum, zin, zcross = R["zsum"], R["zin"], R["zcross"]
        left = z < half
        inward = jnp.where(left, z + 1, z - 1)
        outward = jnp.where(left, z - 1, z + 1)
        edge = (z == 0) | (z == ntp - 1)
        center = (z == half - 1) | (z == half)

        def up(i):
            return rcopy(zsum.at[i], zin.at[i], R["zi_s"].at[i], R["zi_r"].at[i], "tp", inward)

        def cross(i):
            return rcopy(zsum.at[i], zcross.at[i], R["zc_s"].at[i], R["zc_r"].at[i], "tp", inward)

        def down(i):
            return rcopy(xo.at[i], xo.at[i], R["zo_s"].at[i], R["zo_r"].at[i], "tp", outward)

        def settle(i, total):
            update = total.astype(bf).astype(f32)
            xo[i] = (res[i * rz:(i + 1) * rz, :].astype(f32) + update).astype(bf)

        def mine(i):
            return acc_s[i * rz:(i + 1) * rz, :]

        def gathered(i):
            up(i).wait_recv()
            return mine(i) + zin[i].astype(f32)

        if ntp == 1:
            for i in range(kz):
                settle(i, mine(i))
        else:
            outer = jnp.logical_not(center)
            if ntp > 2:
                @pl.when(edge)
                def _():
                    for i in range(kz):
                        zsum[i] = mine(i).astype(bf)
                        up(i).start()

            if ntp > 4:
                @pl.when(outer & jnp.logical_not(edge))
                def _():
                    for i in range(kz):
                        zsum[i] = gathered(i).astype(bf)
                        up(i).start()

            if ntp > 2:
                @pl.when(outer)
                def _():
                    for i in range(kz):
                        down(i).wait_recv()
                        if ntp > 4:
                            @pl.when(jnp.logical_not(edge))
                            def _():
                                down(i).start()
                    for i in range(kz):
                        up(i).wait_send()
                        if ntp > 4:
                            @pl.when(jnp.logical_not(edge))
                            def _():
                                down(i).wait_send()

            @pl.when(center)
            def _():
                lag = 3
                for i in range(kz + lag):
                    if i < kz:
                        zsum[i] = (gathered(i) if ntp > 2 else mine(i)).astype(bf)
                        cross(i).start()
                    if i >= lag:
                        cross(i - lag).wait_recv()
                        settle(i - lag, zsum[i - lag].astype(f32) + zcross[i - lag].astype(f32))
                        if ntp > 2:
                            down(i - lag).start()
                for i in range(kz):
                    cross(i).wait_send()
                    if ntp > 2:
                        down(i).wait_send()

    def dense_rows(d):
        flat = xo[...].reshape(live_rows, feats)
        return lax.dot_general(sel_s[d], flat, (((0,), (0,)), ((), ())), preferred_element_type=f32)

    if do_in:
        ob, og, oaux, aux_s = R["ob"], R["og"], R["oaux"], R["aux_s"]
        snd, loc, r1, s2, r2 = R["snd"], R["loc"], R["r1"], R["s2"], R["r2"]
        chunks, piece, width = snd.shape[2:]
        own = chunks * piece
        r = lax.broadcasted_iota(jnp.int32, (own, own), 0)
        c = lax.broadcasted_iota(jnp.int32, (own, own), 1)
        aux_copies = []
        weights = (R["wb_s"], R["wg_s"])
        pending = list(loads[1:] if do_out else loads)

        def inner(d):
            rows = dense_rows(d) if do_out else R["tok"][d].astype(f32)
            square = jnp.sum(rows * rows, axis=1, keepdims=True)
            aux_s[d, 0:1, :own] = jnp.sum(jnp.where(r == c, square, 0.0), axis=0, keepdims=True)
            aux_s[d, 1:2, :own] = auxin[me, 1:2, :own] if do_out else R["cnt"][...]
            return (rows * R["gain"][li:li + 1, :]).astype(bf)

        def product(k, rows):
            if len(pending) > 1 - k:
                pending.pop(0).wait()
            return jnp.dot(rows, weights[k][...], preferred_element_type=f32).astype(bf)

        def tell(d, g, i):
            aux_copies.append(start(rcopy(aux_s.at[d], oaux.at[me], R["ax_s"].at[g, i],
                                          R["ax_r"].at[g, i], "dp", d)))

        first = {}
        second = {}
        for g in range(nx):
            far = (x + 1 + g) % nx
            rows = inner(2 * far + 1 - core)
            for k in range(2):
                snd[g, k] = product(k, rows).reshape(chunks, piece, width)
                if not do_out and g == 0 and k == 0:
                    pl.semaphore_wait(barrier, greeted)
                for i in range(chunks):
                    first[g, k, i] = start(rcopy(snd.at[g, k, i], r1.at[g, k, i], R["r1_s"].at[g, k, i],
                                                 R["r1_r"].at[g, k, i], "dp", partner))
            tell(2 * far + 1 - core, g, 1)
            rows = inner(2 * far + core)
            if g < nx - 1:
                tell(2 * far + core, g, 0)
            else:
                oaux[me] = aux_s[me]
            for k in range(2):
                loc[g, k] = product(k, rows).reshape(chunks, piece, width)
                if g < nx - 1:
                    for i in range(chunks):
                        first[g, k, i].wait_recv()
                        s2[g, k, i] = (loc[g, k, i].astype(f32) + r1[g, k, i].astype(f32)).astype(bf)
                        second[g, k, i] = start(rcopy(s2.at[g, k, i], r2.at[g, k, i],
                                                      R["r2_s"].at[g, k, i], R["r2_r"].at[g, k, i],
                                                      "dp", 2 * far + core))
        for k, out in ((0, ob), (1, og)):
            for i in range(chunks):
                first[nx - 1, k, i].wait_recv()
                total = loc[nx - 1, k, i].astype(f32) + r1[nx - 1, k, i].astype(f32)
                for g in range(nx - 1):
                    second[g, k, i].wait_recv()
                    total = total + r2[g, k, i].astype(f32)
                out[i] = total
        for cp in aux_copies:
            cp.wait_recv()
    else:
        result, tok = R["result"], R["tok"]
        ones = jnp.ones((live_rows, 128), bf)
        for d in range(ndp):
            hit = lax.dot_general(sel_s[d], ones, (((0,), (0,)), ((), ())), preferred_element_type=f32)
            result[d] = jnp.where(hit[:, 0:1] > 0.5, dense_rows(d).astype(bf), tok[d])
    for cp in sent:
        cp.wait_send()


def bridge(ndp, ntp, steps, own, lanes, live_rows, name, cid, lo=None, li=None, mixed=None, auxin=None,
           w_out=None, tok=None, res=None, gain=None, cnt=None, w_branch=None, w_gate=None):
    f32 = jnp.float32
    bf = jnp.bfloat16
    do_out = mixed is not None
    do_in = w_branch is not None
    nx = ndp // 2
    far = max(nx - 1, 1)
    feats = tok.shape[-1]
    width = mixed.shape[-1] if do_out else w_branch.shape[-1]
    chunks = 4 if own % 64 == 0 else 1
    piece = own // chunks
    kz = 8 if live_rows % 128 == 0 else 1
    rz = live_rows // kz
    anyspace = pl.BlockSpec(memory_space=pl.ANY)
    sem = pltpu.SemaphoreType.DMA
    names, args, specs = [], [], []

    def take(key, a, spec=VM):
        names.append(key)
        args.append(a)
        specs.append(spec)

    dense_res = do_out and res is None
    take("tok", tok)
    if do_out:
        take("m", mixed.reshape(chunks, piece, width))
        take("auxin", auxin)
        take("wo", w_out, anyspace)
        if not dense_res:
            take("res", res)
    if do_in:
        take("gain", gain)
        take("wb", w_branch, anyspace)
        take("wg", w_gate, anyspace)
        if not do_out:
            take("cnt", cnt)
    outs = []
    scratch = []

    def give(key, shape, dtype):
        names.append(key)
        outs.append(jax.ShapeDtypeStruct(shape, dtype))

    if do_out and do_in:
        give("xo", (kz, rz, feats), bf)
    if do_in:
        give("ob", (chunks, piece, width), f32)
        give("og", (chunks, piece, width), f32)
        give("oaux", (ndp, 8, lanes), f32)
    else:
        give("result", (ndp, own, feats), bf)

    def room(key, shape, dtype):
        names.append(key)
        scratch.append(pltpu.VMEM(shape, dtype))

    def sems(key, shape):
        for end in ("_s", "_r"):
            names.append(key + end)
            scratch.append(sem(shape))

    def flag(key):
        names.append(key)
        scratch.append(sem)

    if do_out:
        if not do_in:
            room("xo", (kz, rz, feats), bf)
        room("got", (nx, 2, chunks, piece, width), bf)
        room("acc", (live_rows, feats), f32)
        room("sel", (ndp, live_rows, own), bf)
        if dense_res:
            room("res_s", (live_rows, feats), bf)
        room("wo_s", w_out.shape[1:], bf)
        flag("wo_m")
        for key in ("zsum", "zin", "zcross"):
            room(key, (kz, rz, feats), bf)
        sems("ga", (far, chunks))
        sems("gf", (far, chunks))
        flag("gp_s")
        flag("gp_r")
        for key in ("zi", "zc", "zo"):
            sems(key, (kz,))
    if do_in:
        for key, a in (("wb", w_branch), ("wg", w_gate)):
            room(key + "_s", a.shape[1:], bf)
            flag(key + "_m")
        room("aux_s", (ndp, 8, lanes), f32)
        for key, groups in (("snd", nx), ("loc", nx), ("r1", nx), ("s2", far), ("r2", far)):
            room(key, (groups, 2, chunks, piece, width), bf)
        sems("r1", (nx, 2, chunks))
        sems("r2", (far, 2, chunks))
        sems("ax", (nx, 2))
    return pl.pallas_call(
        functools.partial(bridge_kernel, ndp, ntp, steps, do_out, do_in, dense_res, lo, li, names),
        out_shape=tuple(outs),
        in_specs=specs,
        out_specs=(VM,) * len(outs),
        scratch_shapes=scratch,
        compiler_params=pltpu.CompilerParams(collective_id=cid, has_side_effects=True),
        name=name,
    )(*args)


def cell_kernel(layer, model, heads, steps, cnt_ref, bi_ref, bf_ref, br_ref, gt_ref, aux_ref,
                ccol_ref, crow_ref, mcol_ref, st_ref, cw_ref, wq_ref, wk_ref, wv_ref, wg_ref,
                og_ref, sg_ref, mem_ref, *rest):
    (mixed_ref, nc_ref, newmem_ref, nmax_ref,
     pad_s, conv_s, q_s, k_s, v_s, num_s, car_s, dec_s, cs_s, top_s, nc_s, stage, ins, outs) = rest[-18:]
    f32 = jnp.float32
    bf = jnp.bfloat16
    batch = stage.shape[0]
    own, width = br_ref.shape
    dim = HEAD_DIM
    base = 8 - (CONV - 1)

    def fetch(b):
        return pltpu.make_async_copy(mem_ref.at[layer, b], stage.at[b], ins.at[b])

    def store(b):
        return pltpu.make_async_copy(stage.at[b], newmem_ref.at[layer, b], outs.at[b])

    for b in range(batch):
        fetch(b).start()

    squares = aux_ref[0, 0:1, :own]
    for i in range(1, aux_ref.shape[0]):
        squares = squares + aux_ref[i, 0:1, :own]
    inv_row = lax.rsqrt(squares / model + epsilon)
    r = lax.broadcasted_iota(jnp.int32, (own, own), 0)
    c = lax.broadcasted_iota(jnp.int32, (own, own), 1)
    inv = jnp.sum(jnp.where(r == c, inv_row, 0.0), axis=1, keepdims=True)
    branch = (br_ref[...] * inv).astype(bf)
    pad_s[:, 8:8 + steps, :] = branch.astype(f32).reshape(batch, steps, width)
    for j in range(CONV - 1):
        rows = st_ref[0, j].astype(f32)
        for b in range(batch):
            pad_s[b, base + j:base + j + 1, :] = rows[b:b + 1, :]
    total = pad_s[:, base:base + steps, :] * cw_ref[0, 0:1, :]
    for j in range(1, CONV):
        total = total + pad_s[:, base + j:base + j + steps, :] * cw_ref[0, j:j + 1, :]
    conv = (total * jax.nn.sigmoid(total)).astype(bf).reshape(own, width)
    conv_s[...] = conv
    for b in range(batch):
        for i in range(CONV - 1):
            nc_s[i, b:b + 1, :] = pad_s[b, pl.ds(base + i + cnt_ref[b], 1), :]
    nc_ref[...] = nc_s[...].astype(bf)

    same = (r // steps) == (c // steps)
    causal = same & (r >= c)
    behind = same & (r <= c)
    live_col = (r[:, 0:1] % steps) < ccol_ref[...]
    live_row = (c[0:1, :] % steps) < crow_ref[...]
    nt = (((1,), (1,)), ((), ()))
    for h in range(heads):
        sl = slice(h * dim, (h + 1) * dim)
        q = jnp.dot(conv[:, sl], wq_ref[0, h], preferred_element_type=f32).astype(bf)
        k = jnp.dot(conv[:, sl], wk_ref[0, h], preferred_element_type=f32).astype(bf)
        v = jnp.dot(branch[:, sl], wv_ref[0, h], preferred_element_type=f32).astype(bf)
        gcol = None
        for i, part in enumerate((q, k, v)):
            w = wg_ref[0, h, :, i * dim:(i + 1) * dim]
            one = lax.dot_general(part, w, nt, preferred_element_type=f32)
            two = lax.dot_general(w, part, nt, preferred_element_type=f32)
            gcol, grow = (one, two) if gcol is None else (gcol + one, grow + two)
        bias_i = bi_ref[layer, h]
        bias_f = bf_ref[layer, h]

        def log_sig(x):
            return jnp.minimum(x, 0.0) - jnp.log1p(jnp.exp(-jnp.abs(x)))

        ig_col = jnp.where(live_col, gcol[:, 0:1] + bias_i, very_negative)
        ig_row = jnp.where(live_row, grow[0:1, :] + bias_i, very_negative)
        fg_col = jnp.where(live_col, log_sig(gcol[:, 1:2] + bias_f), 0.0)
        fg_row = jnp.where(live_row, log_sig(grow[1:2, :] + bias_f), 0.0)
        cum_col = jnp.sum(jnp.where(causal, fg_row, 0.0), axis=1, keepdims=True)
        end_col = jnp.sum(jnp.where(same, fg_row, 0.0), axis=1, keepdims=True)
        cum_row = jnp.sum(jnp.where(behind, fg_col, 0.0), axis=0, keepdims=True)
        lift_row = ig_row - cum_row
        logw = jnp.where(causal, cum_col + lift_row, very_negative)
        old_max = mcol_ref[:, h:h + 1]
        carried = cum_col + old_max
        stab = jnp.maximum(jnp.max(logw, axis=1, keepdims=True), carried)
        weights = jnp.exp(logw - stab)
        top = jnp.max(jnp.where(same, end_col + lift_row, very_negative), axis=1, keepdims=True)
        new_max = jnp.maximum(top, end_col + old_max)
        update = jnp.exp(end_col - cum_col + ig_col - new_max)
        top_s[:, h:h + 1] = new_max
        dec_s[:, h:h + 1] = jnp.exp(end_col + old_max - new_max)
        cs_s[:, h:h + 1] = jnp.exp(carried - stab)
        scores = lax.dot_general(q, k, nt, preferred_element_type=f32)
        scores = (jnp.where(causal, scores, 0.0) * (dim ** -0.5) * weights).astype(bf)
        num_s[:, sl] = jnp.dot(scores, v, preferred_element_type=f32)
        q_s[:, sl] = q.astype(f32)
        k_s[:, sl] = k.astype(f32) * (dim ** -0.5) * update
        v_s[:, sl] = v.astype(f32)
    nmax_ref[...] = top_s[pl.ds(steps - 1, batch, stride=steps), :]

    @pl.loop(0, batch)
    def _(b):
        fetch(b).wait()
        rows = pl.ds(pl.multiple_of(b * steps, 8), steps)
        for h in range(heads):
            sl = slice(h * dim, (h + 1) * dim)
            old = stage[b, h]
            car_s[rows, sl] = jnp.dot(q_s[rows, sl].astype(bf), old.astype(bf), preferred_element_type=f32)
            outer = lax.dot_general(
                k_s[rows, sl].astype(bf), v_s[rows, sl].astype(bf), (((0,), (0,)), ((), ())),
                preferred_element_type=f32,
            )
            stage[b, h] = dec_s[rows, :][0:1, h:h + 1] * old + outer
        store(b).start()

    live = (lax.broadcasted_iota(jnp.int32, (own, 1), 0) % steps) < ccol_ref[...]
    for h in range(heads):
        sl = slice(h * dim, (h + 1) * dim)
        num = num_s[:, sl] + cs_s[:, h:h + 1] * car_s[:, sl]
        centered = num - jnp.mean(num, axis=1, keepdims=True)
        normal = centered * lax.rsqrt(jnp.mean(centered * centered, axis=1, keepdims=True) + epsilon)
        gate = (gt_ref[:, sl] * inv).astype(bf).astype(f32)
        mixed = normal * og_ref[0, h:h + 1, :] + sg_ref[layer:layer + 1, sl] * conv_s[:, sl].astype(f32)
        mixed = mixed * (gate * jax.nn.sigmoid(gate))
        mixed_ref[:, sl] = jnp.where(live, mixed, 0.0).astype(bf)
    for b in range(batch):
        store(b).wait()


def memory_cell(layer, model, steps, counts, bias_input, bias_forget, branch, gate, aux, count_col,
                count_row, old_max, state, conv_weight, w_query, w_key, w_value, w_gates, out_gain,
                skip_gain, memory, previous):
    _, batch, heads, dim, _ = memory.shape
    own, width = branch.shape
    f32 = jnp.float32

    def whole(a):
        return pl.BlockSpec(a.shape, lambda i: (0,) * a.ndim)

    def layered(a):
        return pl.BlockSpec((1,) + a.shape[1:], lambda i: (layer,) + (0,) * (a.ndim - 1))

    smem = pl.BlockSpec(memory_space=pltpu.SMEM)
    anyspace = pl.BlockSpec(memory_space=pl.ANY)
    args = [counts, bias_input, bias_forget, branch, gate, aux, count_col, count_row, old_max,
            state, conv_weight, w_query, w_key, w_value, w_gates, out_gain, skip_gain, memory]
    specs = [smem, smem, smem] + [whole(a) for a in args[3:9]] + [layered(a) for a in args[9:16]]
    specs += [whole(skip_gain), anyspace]
    aliases = {}
    if previous is not None:
        aliases = {len(args): 2}
        args.append(previous)
        specs.append(anyspace)
    big = pltpu.VMEM((own, width), f32)
    small = pltpu.VMEM((own, 128), f32)
    return pl.pallas_call(
        functools.partial(cell_kernel, layer, model, heads, steps),
        grid=(1,),
        out_shape=(
            jax.ShapeDtypeStruct((own, width), jnp.bfloat16),
            jax.ShapeDtypeStruct((CONV - 1, batch, width), jnp.bfloat16),
            jax.ShapeDtypeStruct(memory.shape, f32),
            jax.ShapeDtypeStruct((batch, 128), f32),
        ),
        in_specs=specs,
        out_specs=(
            pl.BlockSpec((own, width), lambda i: (0, 0)),
            pl.BlockSpec((CONV - 1, batch, width), lambda i: (0, 0, 0)),
            anyspace,
            pl.BlockSpec((batch, 128), lambda i: (0, 0)),
        ),
        scratch_shapes=[
            pltpu.VMEM((batch, 8 + steps, width), f32),
            pltpu.VMEM((own, width), jnp.bfloat16),
            big, big, big, big, big, small, small, small,
            pltpu.VMEM((CONV - 1, batch, width), f32),
            pltpu.VMEM((batch, heads, dim, dim), f32),
            pltpu.SemaphoreType.DMA((batch,)), pltpu.SemaphoreType.DMA((batch,)),
        ],
        input_output_aliases=aliases,
        compiler_params=pltpu.CompilerParams(dimension_semantics=("arbitrary",)),
        name="memory_cell",
    )(*args)


def per_device(tokens, live_counts, norm_gain, w_branch, w_silu_gate, conv_weight, w_query, w_key,
               w_value, w_input_gate, w_forget_gate, bias_input, bias_forget, out_gain, skip_gain,
               w_out, conv_state, memory, max_state):
    f32 = jnp.float32
    ndp = lax.axis_size("dp")
    ntp = lax.axis_size("tp")
    all_batch, steps, features = tokens.shape
    batch = live_counts.shape[0]
    width = w_branch.shape[2]
    heads = w_query.shape[1]
    own = batch * steps
    live_rows = all_batch * steps // 2
    lanes = -(-own // 128) * 128
    model = features * ndp
    flat = tokens.reshape(ndp, own, features)
    repeated = jnp.repeat(live_counts, steps)
    count_col = repeated[:, None]
    count_row = repeated[None, :]
    old_max = jnp.repeat(max_state, steps, axis=1)
    states = jnp.transpose(conv_state, (0, 2, 1, 3))
    w_gates = jnp.pad(jnp.stack([w_input_gate, w_forget_gate], axis=2), ((0, 0), (0, 0), (0, 6), (0, 0)))
    link = functools.partial(bridge, ndp, ntp, steps, own, lanes, live_rows)

    branch, gate, aux = link("enter", 0, li=0, tok=flat, gain=norm_gain, cnt=count_row.astype(f32),
                             w_branch=w_branch, w_gate=w_silu_gate)
    new_memory = None
    compact = None
    conv_list = []
    max_list = []
    for l in range(LAYERS):
        mixed, new_conv, new_memory, new_max = memory_cell(
            l, model, steps, live_counts, bias_input, bias_forget, branch.reshape(own, width),
            gate.reshape(own, width), aux, count_col, count_row, old_max[l], states, conv_weight,
            w_query, w_key, w_value, w_gates, out_gain, skip_gain, memory, new_memory
        )
        conv_list.append(new_conv)
        max_list.append(new_max[:, :heads])
        if l + 1 < LAYERS:
            compact, branch, gate, aux = link(
                f"bridge{l}", l + 1, lo=l, li=l + 1, mixed=mixed, auxin=aux, w_out=w_out, tok=flat,
                res=compact, gain=norm_gain, w_branch=w_branch, w_gate=w_silu_gate
            )
            compact = compact.reshape(live_rows, features)
        else:
            (result,) = link("leave", l + 1, lo=l, mixed=mixed, auxin=aux, w_out=w_out, tok=flat, res=compact)
    new_conv = jnp.transpose(jnp.stack(conv_list), (0, 2, 1, 3))
    return (result.reshape(tokens.shape), new_conv, new_memory, jnp.stack(max_list))


def solution(mesh):
    in_specs = (
        P("grp", None, "dp"),
        P(("grp", "dp")),
        P(None, "dp"),
        P(None, "dp", "tp"),
        P(None, "dp", "tp"),
        P(None, None, "tp"),
        P(None, "tp", None, None),
        P(None, "tp", None, None),
        P(None, "tp", None, None),
        P(None, "tp", None),
        P(None, "tp", None),
        P(None, "tp"),
        P(None, "tp"),
        P(None, "tp", None),
        P(None, "tp"),
        P(None, "tp", "dp"),
        P(None, ("grp", "dp"), None, "tp"),
        P(None, ("grp", "dp"), "tp", None, None),
        P(None, ("grp", "dp"), "tp"),
    )
    out_specs = (
        P("grp", None, "dp"),
        P(None, ("grp", "dp"), None, "tp"),
        P(None, ("grp", "dp"), "tp", None, None),
        P(None, ("grp", "dp"), "tp"),
    )
    return jax.shard_map(
        per_device, mesh=mesh, in_specs=in_specs, out_specs=out_specs, check_vma=False
    )
```

time: 160 us -> 137 us (0.86)
  matrix products: 18.9 us -> 0 us
  Pallas kernels: 130 us -> 124 us
  local copies, waits for them, and re-layouts: 6.09 us -> 8.52 us
    dot_general x9 -> x0, matrix products: 18.9 us -> none  [the longest x2 5.92 us: per_device(): part = jnp.dot(packed, w_out[l], preferred_element_type=f32).astype(bf)]
    pallas_call x6 -> x3, Pallas kernels: 96.5 us -> 90.3 us  [bridge(): pl.pallas_call(functools.partial(bridge_kernel, ndp, ntp, steps, do_out,...]
    unnamed x18 -> x5, local copies, waits for them, and re-layouts: 0.04 us -> 1.88 us
where the time goes in v2:
time: 137 us
  Pallas kernels  124 us (91%)
  local copies, waits for them, and re-layouts  8.52 us (6%)
  other arithmetic  3.41 us (2%)
    pallas_call x3, Pallas kernels, bridge(): pl.pallas_call(functools.partial(bridge_kernel, ndp, ntp, steps, do_out,...  90.3 us
    pallas_call x2, Pallas kernels, memory_cell(): pl.pallas_call(functools.partial(cell_kernel, layer, model, heads, steps)...  33.8 us

profile of v2, /device:TPU:0, one launch (start us, length us, event | category | flops | bytes accessed | tf_op | source)
XLA Modules:
  0.0 136.8 jit_solution(7457883724338898910)
XLA Ops:
  0.6 0.7 slice_bitcast_fusion
  1.3 0.1 copy.34
  1.4 0.7 broadcast_in_dim.12
  2.1 0.1 broadcast_in_dim_reshape.6.crow_ref
  2.2 0.0 copy-start.1
  2.2 0.5 convert_element_type.5.refs_4_
  2.8 0.1 copy.30
  2.8 0.7 copy.31
  3.6 0.7 copy.32
  4.3 0.7 fusion.2.wg_ref
  5.0 0.7 broadcast_in_dim_reshape.8.ccol_ref
  5.7 0.6 broadcast_bitcast_fusion.1.mcol_ref
  6.3 0.6 broadcast_bitcast_fusion.mcol_ref
  7.0 20.5 %enter.1 = (f32[4,32,1024]{2,1,0:T(8,128)}, f32[4,32,1024]{2,1,0:T(8,128)}, f32[4,8,128]{2,1,0:T(8,128)}) custom-call(bf16[4,128,512]{2,1,0:T(8,128)(2,1)} %bitcast.28, f32[2,512]{1,0:T(2,128)} %refs_4_.1, bf16[2,512,1024]{2,1,0:T(8,128)(2,1)} %refs_5_.1, bf16[2,512,1024]{2,1,0:T(8,128)(2,1)} %refs_6_.1, f32[1,128]{1,0:T(1,128)} %convert_element_type.5.refs_4_), custom_call_target="tpu_custom_call" | custom-call | tf_op jit(solution)/shard_map/enter/pallas_call | solution.py:379
  27.5 0.0 copy-done.1
  27.5 16.6 %memory_cell.2 = (bf16[128,1024]{1,0:T(8,128)(2,1)}, bf16[3,16,1024]{2,1,0:T(8,128)(2,1)}, f32[2,16,4,256,256]{4,3,2,1,0:T(8,128)}, f32[16,128]{1,0:T(8,128)}) custom-call(s32[16]{0:T(128)} %cnt_ref.3, f32[2,4]{1,0:T(2,128)} %bi_ref.3, f32[2,4]{1,0:T(2,128)} %bf_ref.3, f32[128,1024]{1,0:T(8,128)} %bitcast.36, f32[128,1024]{1,0:T(8,128)} %bitcast.37, ...), custom_call_target="tpu_custom_call" | custom-call | tf_op jit(solution)/shard_map/memory_cell/pallas_call | solution.py:539
  44.1 0.8 copy.36
  44.9 43.1 %bridge0.1 = (bf16[8,32,512]{2,1,0:T(8,128)(2,1)}, f32[4,32,1024]{2,1,0:T(8,128)}, f32[4,32,1024]{2,1,0:T(8,128)}, f32[4,8,128]{2,1,0:T(8,128)}) custom-call(bf16[4,128,512]{2,1,0:T(8,128)(2,1)} %bitcast.29, bf16[4,32,1024]{2,1,0:T(8,128)(2,1)} %bitcast.40, f32[4,8,128]{2,1,0:T(8,128)} %get-tuple-element.21.aux_ref.refs_2_, bf16[2,1024,512]{2,1,0:T(8,128)(2,1)} %refs_3_.5, ...), custom_call_target="tpu_custom_call" | custom-call | tf_op jit(solution)/shard_map/bridge0/pallas_call | solution.py:379
  88.0 0.0 copy-start
  88.0 17.2 %memory_cell.3 = (bf16[128,1024]{1,0:T(8,128)(2,1)}, bf16[3,16,1024]{2,1,0:T(8,128)(2,1)}, f32[2,16,4,256,256]{4,3,2,1,0:T(8,128)}, f32[16,128]{1,0:T(8,128)}) custom-call(s32[16]{0:T(128)} %cnt_ref.3, f32[2,4]{1,0:T(2,128)} %bi_ref.3, f32[2,4]{1,0:T(2,128)} %bf_ref.3, f32[128,1024]{1,0:T(8,128)} %bitcast.34, ...), custom_call_target="tpu_custom_call", output_to_operand_aliasing={{2}: (18, {})} | custom-call | tf_op jit(solution)/shard_map/memory_cell/pallas_call | solution.py:539
  105.2 26.7 %leave.1 = bf16[4,128,512]{2,1,0:T(8,128)(2,1)} custom-call(bf16[4,128,512]{2,1,0:T(8,128)(2,1)} %bitcast.30, bf16[4,32,1024]{2,1,0:T(8,128)(2,1)} %bitcast.39, f32[4,8,128]{2,1,0:T(8,128)} %get-tuple-element.25.aux_ref.refs_2_, bf16[2,1024,512]{2,1,0:T(8,128)(2,1)} %refs_3_.5, bf16[256,512]{1,0:T(8,128)(2,1)} %bitcast.38), custom_call_target="tpu_custom_call" | custom-call | tf_op jit(solution)/shard_map/leave/pallas_call | solution.py:379
  131.9 0.0 copy-done
  131.9 1.6 %maximum_bitcast_fusion = bf16[2,16,3,1024]{3,1,2,0:T(8,128)(2,1)} fusion(bf16[1,3,16,1024]{3,2,1,0:T(8,128)(2,1)} %bitcast.42, bf16[1,3,16,1024]{3,2,1,0:T(8,128)(2,1)S(1)} %bitcast.41), kind=kLoop, calls=%fused_computation.3 | loop fusion | flops 98304 | bytes 393216 | tf_op jit(solution)/shard_map/transpose | solution.py:614
  133.5 0.8 copy.37
  134.3 0.6 pad_maximum_fusion
  134.9 1.9 %copy.40 = bf16[64,8,512]{2,1,0:T(8,128)(2,1)} copy(bf16[64,8,512]{2,1,0:T(8,128)(2,1)} %bitcast.31) | data formatting | bytes 1048576
Async XLA Ops:
  2.2 25.2 %copy-start.1 = (s32[1,128]{1,0:T(1,128)}, s32[1,128]{1,0:T(1,128)S(1)}, u32[]{:S(2)}) copy-start(s32[1,128]{1,0:T(1,128)S(1)} %broadcast_in_dim_reshape.6.crow_ref) | copy-start | bytes 1540
  88.0 43.9 %copy-start = (bf16[3,16,1024]{2,1,0:T(8,128)(2,1)S(1)}, bf16[3,16,1024]{2,1,0:T(8,128)(2,1)}, u32[]{:S(2)}) copy-start(bf16[3,16,1024]{2,1,0:T(8,128)(2,1)} %get-tuple-element.29) | copy-start | bytes 294916

commit v3 on v2

v3 whole, which is shorter than its diff:
```python
import functools

import jax
import jax.numpy as jnp
from jax import lax
from jax.experimental import pallas as pl
from jax.experimental.pallas import tpu as pltpu
from jax.sharding import PartitionSpec as P

HEAD_DIM = 256
CONV = 4
LAYERS = 2
epsilon = 1e-06
very_negative = -1e30

FULL_VMEM = 60 * 1024 * 1024
LEAVE_VMEM = 24 * 1024 * 1024

VM = pl.BlockSpec(memory_space=pltpu.VMEM)
MESH = pl.DeviceIdType.MESH


def rcopy(src, dst, send, recv, axis, device):
    return pltpu.make_async_remote_copy(
        src_ref=src, dst_ref=dst, send_sem=send, recv_sem=recv,
        device_id={axis: device}, device_id_type=MESH,
    )


def bridge_kernel(ndp, ntp, do_out, do_in, lo, li, names, *refs):
    R = dict(zip(names, refs))
    f32 = jnp.float32
    bf = jnp.bfloat16
    nx = ndp // 2
    me = lax.axis_index("dp")
    core = me % 2
    x = me // 2
    partner = me + 1 - 2 * core
    z = lax.axis_index("tp")
    tok = R["tok"]
    chunks, piece, feats = tok.shape[1:]
    own = chunks * piece
    halves = 2 if chunks > 1 else 1
    step = chunks // halves
    pieces = {}
    for h in range(halves):
        pieces[h] = list(range(h * step, (h + 1) * step))

    def load(name, layer):
        return pltpu.make_async_copy(R[name].at[layer], R[name + "_s"], R[name + "_m"])

    wanted = ([("wo", lo)] if do_out else []) + ([("wb", li), ("wg", li)] if do_in else [])
    for name, layer in wanted:
        load(name, layer).start()
    barrier = pltpu.get_barrier_semaphore()
    for off in range(1, ndp):
        pl.semaphore_signal(barrier, inc=1, device_id={"dp": (me + off) % ndp}, device_id_type=MESH)
    greeted = ndp - 1
    if do_out and ntp > 1:
        @pl.when(z > 0)
        def _():
            pl.semaphore_signal(barrier, inc=1, device_id={"tp": z - 1}, device_id_type=MESH)

        @pl.when(z < ntp - 1)
        def _():
            pl.semaphore_signal(barrier, inc=1, device_id={"tp": z + 1}, device_id_type=MESH)
        greeted = greeted + jnp.where(z > 0, 1, 0) + jnp.where(z < ntp - 1, 1, 0)
    pl.semaphore_wait(barrier, greeted)

    def ahead(g):
        return (x + 1 + g) % nx

    def behind(g):
        return (x + nx - 1 - g) % nx

    groups = [("mine", nx - 1, h) for h in range(halves)]
    groups += [("other", nx - 1, 0)]
    for g in range(nx - 1):
        for h in range(halves):
            groups += [("mine", g, h), ("other", g, h)]
    groups += [("other", nx - 1, h) for h in range(1, halves)]
    if not do_out:
        groups = [(kind, g, h) for g in range(nx) for h in range(halves) for kind in ("other", "mine")]

    if do_out:
        m_ref, got, psum = R["m"], R["got"], R["psum"]
        width = m_ref.shape[2]
        fresh = R["fresh"]

        def device(kind, g):
            if g == nx - 1:
                return me if kind == "mine" else partner
            return 2 * behind(g) + (core if kind == "mine" else 1 - core)

        def across(g, c):
            return rcopy(m_ref.at[c], got.at[x, core, c], R["ga_s"].at[g, c], R["ga_r"].at[g, c],
                         "dp", 2 * ahead(g) + core)

        def near(c):
            return rcopy(m_ref.at[c], got.at[x, core, c], R["gp_s"].at[c], R["gp_r"].at[c],
                         "dp", partner)

        def passed(g, c):
            spot = got.at[behind(g), core, c]
            return rcopy(spot, spot, R["gf_s"].at[g, c], R["gf_r"].at[g, c], "dp", partner)

        for c in range(chunks):
            for g in range(nx - 1):
                across(g, c).start()
        for c in range(chunks):
            near(c).start()
        load("wo", lo).wait()

        def rows_of(kind, g, h):
            if g == nx - 1:
                if kind == "mine":
                    return m_ref[h * step:(h + 1) * step]
                for c in pieces[h]:
                    near(c).wait_recv()
                return got[x, 1 - core, h * step:(h + 1) * step]
            if kind == "mine":
                for c in pieces[h]:
                    across(g, c).wait_recv()
                    passed(g, c).start()
                return got[behind(g), core, h * step:(h + 1) * step]
            for c in pieces[h]:
                passed(g, c).wait_recv()
            return got[behind(g), 1 - core, h * step:(h + 1) * step]

        def product_out(i):
            rows = rows_of(*groups[i]).reshape(step * piece, width)
            part = jnp.dot(rows, R["wo_s"][...], preferred_element_type=f32)
            psum[i * step:(i + 1) * step] = part.reshape(step, piece, feats)

        half = ntp // 2
        zsum, zin, zcross = R["zsum"], R["zin"], R["zcross"]
        left = z < half
        inward = jnp.where(left, z + 1, z - 1)
        outward = jnp.where(left, z - 1, z + 1)
        edge = (z == 0) | (z == ntp - 1)
        center = (z == half - 1) | (z == half)
        inner = jnp.logical_not(edge)
        outer = jnp.logical_not(center)
        spots = len(groups) * step

        def spot_of(p):
            kind, g, h = groups[p // step]
            return device(kind, g), h * step + p % step

        def up(p):
            return rcopy(zsum.at[p], zin.at[p], R["zi_s"].at[p], R["zi_r"].at[p], "tp", inward)

        def cross(p):
            return rcopy(zsum.at[p], zcross.at[p], R["zc_s"].at[p], R["zc_r"].at[p], "tp", inward)

        def down(p):
            d, c = spot_of(p)
            return rcopy(fresh.at[d, c], fresh.at[d, c], R["zo_s"].at[p], R["zo_r"].at[p], "tp", outward)

        def settle(p, total):
            d, c = spot_of(p)
            update = total.astype(bf).astype(f32)
            fresh[d, c] = (tok[d, c].astype(f32) + update).astype(bf)

        def gathered(p):
            up(p).wait_recv()
            return psum[p] + zin[p].astype(f32)

    if do_in:
        ob, og, oaux, aux_s = R["ob"], R["og"], R["oaux"], R["aux_s"]
        snd, loc, r1, s2, r2 = R["snd"], R["loc"], R["r1"], R["s2"], R["r2"]
        wide = snd.shape[-1]
        weights = (R["wb_s"], R["wg_s"])
        source = fresh if do_out else tok
        aux_s[...] = jnp.zeros_like(aux_s)

        def target(kind, g):
            if g == nx - 1:
                return me if kind == "mine" else partner
            return 2 * ahead(g) + (core if kind == "mine" else 1 - core)

        def first(g, k, c):
            return rcopy(snd.at[g, k, c], r1.at[g, k, c], R["r1_s"].at[g, k, c], R["r1_r"].at[g, k, c],
                         "dp", partner)

        def second(g, k, c):
            return rcopy(s2.at[g, k, c], r2.at[g, k, c], R["r2_s"].at[g, k, c], R["r2_r"].at[g, k, c],
                         "dp", 2 * ahead(g) + core)

        def tell(kind, g):
            d = target(kind, g)
            i = 0 if kind == "mine" else 1
            return rcopy(aux_s.at[d], oaux.at[me], R["ax_s"].at[g, i], R["ax_r"].at[g, i], "dp", d)

        def forward(g, h):
            for k in range(2):
                for c in pieces[h]:
                    first(g, k, c).wait_recv()
                    s2[g, k, c] = (loc[g, k, c].astype(f32) + r1[g, k, c].astype(f32)).astype(bf)
                    second(g, k, c).start()

        def handle(kind, g, h, done, waiting):
            gw = g
            if do_out and g < nx - 1:
                gw = nx - 2 - g
            d = target(kind, gw)
            size = step * piece
            rows = source[d, h * step:(h + 1) * step].reshape(size, feats).astype(f32)
            square = jnp.sum(rows * rows, axis=1, keepdims=True)
            r = lax.broadcasted_iota(jnp.int32, (size, own), 0) + h * size
            c = lax.broadcasted_iota(jnp.int32, (size, own), 1)
            line = jnp.sum(jnp.where(r == c, square, 0.0), axis=0, keepdims=True)
            if h == 0:
                aux_s[d, 0:1, :own] = line
            else:
                aux_s[d, 0:1, :own] += line
            done.append((kind, gw))
            scaled = (rows * R["gain"][li:li + 1, :]).astype(bf)
            for k in range(2):
                part = jnp.dot(scaled, weights[k][...], preferred_element_type=f32).astype(bf)
                part = part.reshape(step, piece, wide)
                if kind == "mine":
                    loc[gw, k, h * step:(h + 1) * step] = part
                else:
                    snd[gw, k, h * step:(h + 1) * step] = part
                    for c in pieces[h]:
                        first(gw, k, c).start()
            if done.count((kind, gw)) == halves:
                if (kind, gw) == ("mine", nx - 1):
                    oaux[me] = aux_s[me]
                else:
                    tell(kind, gw).start()
            while waiting:
                forward(*waiting.pop(0))
            if gw < nx - 1:
                pair = [(a, gw, h) for a in ("mine", "other")]
                done.append(("seen", kind, gw, h))
                if all(("seen",) + a in done for a in pair):
                    waiting.append((gw, h))

        def flush(waiting):
            while waiting:
                forward(*waiting.pop(0))

    if do_in:
        for name in ("wb", "wg"):
            load(name, li).wait()
    if not do_out:
        done, waiting = [], []
        for group in groups:
            handle(*group, done, waiting)
        flush(waiting)
    else:
        def finish(i, done, waiting):
            if do_in:
                handle(*groups[i], done, waiting)

        if ntp == 1:
            done, waiting = [], []
            for i in range(len(groups)):
                product_out(i)
                for p in range(i * step, (i + 1) * step):
                    settle(p, psum[p])
                finish(i, done, waiting)
            if do_in:
                flush(waiting)
        else:
            if ntp > 2:
                @pl.when(outer)
                def _():
                    done, waiting = [], []
                    for i in range(len(groups)):
                        product_out(i)
                        for p in range(i * step, (i + 1) * step):
                            if ntp == 4:
                                zsum[p] = psum[p].astype(bf)
                            else:
                                @pl.when(edge)
                                def _():
                                    zsum[p] = psum[p].astype(bf)

                                @pl.when(inner)
                                def _():
                                    zsum[p] = gathered(p).astype(bf)
                            up(p).start()
                    for i in range(len(groups)):
                        for p in range(i * step, (i + 1) * step):
                            down(p).wait_recv()
                            if ntp > 4:
                                @pl.when(inner)
                                def _():
                                    down(p).start()
                        finish(i, done, waiting)
                    if do_in:
                        flush(waiting)
                    for p in range(spots):
                        up(p).wait_send()
                        if ntp > 4:
                            @pl.when(inner)
                            def _():
                                down(p).wait_send()

            @pl.when(center)
            def _():
                done, waiting = [], []
                lag = 3
                for p in range(spots + lag):
                    if p < spots:
                        if p % step == 0:
                            product_out(p // step)
                        zsum[p] = (gathered(p) if ntp > 2 else psum[p]).astype(bf)
                        cross(p).start()
                    q = p - lag
                    if q >= 0:
                        cross(q).wait_recv()
                        settle(q, zsum[q].astype(f32) + zcross[q].astype(f32))
                        if ntp > 2:
                            down(q).start()
                        if q % step == step - 1:
                            finish(q // step, done, waiting)
                if do_in:
                    flush(waiting)
                for p in range(spots):
                    cross(p).wait_send()
                    if ntp > 2:
                        down(p).wait_send()

        for c in range(chunks):
            near(c).wait_send()
            for g in range(nx - 1):
                across(g, c).wait_send()
                passed(g, c).wait_send()

    if do_in:
        last = nx - 1
        for g in range(nx):
            for i, kind in enumerate(("mine", "other")):
                if (kind, g) != ("mine", last):
                    tell(kind, g).wait_recv()
        total = oaux[0, 0:1, :own]
        for d in range(1, ndp):
            total = total + oaux[d, 0:1, :own]
        inv_row = lax.rsqrt(total / (feats * ndp) + epsilon)
        r = lax.broadcasted_iota(jnp.int32, (own, own), 0)
        c = lax.broadcasted_iota(jnp.int32, (own, own), 1)
        inv = jnp.sum(jnp.where(r == c, inv_row, 0.0), axis=1, keepdims=True)
        for h in range(halves):
            for k, out in ((0, ob), (1, og)):
                for c in pieces[h]:
                    first(last, k, c).wait_recv()
                    total = loc[last, k, c].astype(f32) + r1[last, k, c].astype(f32)
                    for g in range(nx - 1):
                        second(g, k, c).wait_recv()
                        total = total + r2[g, k, c].astype(f32)
                    out[c * piece:(c + 1) * piece, :] = (
                        total * inv[c * piece:(c + 1) * piece, :]
                    ).astype(bf)
        for g in range(nx):
            for kind in ("mine", "other"):
                if (kind, g) != ("mine", last):
                    tell(kind, g).wait_send()
            for k in range(2):
                for c in range(chunks):
                    first(g, k, c).wait_send()
                    if g < last:
                        second(g, k, c).wait_send()


def bridge(ndp, ntp, lanes, name, cid, limit, tok, lo=None, li=None, mixed=None, w_out=None, gain=None,
           w_branch=None, w_gate=None):
    f32 = jnp.float32
    bf = jnp.bfloat16
    do_out = mixed is not None
    do_in = w_branch is not None
    nx = ndp // 2
    far = max(nx - 1, 1)
    chunks, piece, feats = tok.shape[1:]
    own = chunks * piece
    spots = ndp * chunks
    weight = pl.BlockSpec(memory_space=pl.ANY)
    sem = pltpu.SemaphoreType.DMA
    names, args, specs, outs, scratch = [], [], [], [], []

    def take(key, a, spec=VM):
        names.append(key)
        args.append(a)
        specs.append(spec)

    take("tok", tok)
    if do_out:
        width = mixed.shape[-1]
        take("m", mixed.reshape(chunks, piece, width))
        take("wo", w_out, weight)
    if do_in:
        width = w_branch.shape[-1]
        take("gain", gain)
        take("wb", w_branch, weight)
        take("wg", w_gate, weight)

    def give(key, shape, dtype):
        names.append(key)
        outs.append(jax.ShapeDtypeStruct(shape, dtype))

    if do_out:
        give("fresh", tok.shape, bf)
    if do_in:
        give("ob", (own, width), bf)
        give("og", (own, width), bf)

    def room(key, shape, dtype):
        names.append(key)
        scratch.append(pltpu.VMEM(shape, dtype))

    def flag(key, *shape):
        names.append(key)
        scratch.append(sem(shape) if shape else sem)

    def sems(key, *shape):
        flag(key + "_s", *shape)
        flag(key + "_r", *shape)

    if do_out:
        room("got", (nx, 2, chunks, piece, width), bf)
        room("psum", (spots, piece, feats), f32)
        room("wo_s", w_out.shape[1:], bf)
        flag("wo_m")
        for key in ("zsum", "zin", "zcross"):
            room(key, (spots, piece, feats), bf)
        sems("ga", far, chunks)
        sems("gf", far, chunks)
        sems("gp", chunks)
        for key in ("zi", "zc", "zo"):
            sems(key, spots)
    if do_in:
        for key, a in (("wb", w_branch), ("wg", w_gate)):
            room(key + "_s", a.shape[1:], bf)
            flag(key + "_m")
        room("aux_s", (ndp, 8, lanes), f32)
        room("oaux", (ndp, 8, lanes), f32)
        for key, count in (("snd", nx), ("loc", nx), ("r1", nx), ("s2", far), ("r2", far)):
            room(key, (count, 2, chunks, piece, width), bf)
        sems("r1", nx, 2, chunks)
        sems("r2", far, 2, chunks)
        sems("ax", nx, 2)
    return pl.pallas_call(
        functools.partial(bridge_kernel, ndp, ntp, do_out, do_in, lo, li, names),
        out_shape=tuple(outs),
        in_specs=specs,
        out_specs=(VM,) * len(outs),
        scratch_shapes=scratch,
        compiler_params=pltpu.CompilerParams(
            collective_id=cid, has_side_effects=True, vmem_limit_bytes=limit
        ),
        name=name,
    )(*args)


def cell_kernel(layer, heads, steps, cnt_ref, bi_ref, bf_ref, cvec_ref, br_ref, gt_ref, mrow_ref, st_ref,
                cw_ref, wi_ref, wf_ref, og_ref, sg_ref, wq_ref, wk_ref, wv_ref, mem_ref, *rest):
    (mixed_ref, nc_ref, newmem_ref, nmax_ref,
     pad_s, conv_s, q_s, k_s, v_s, num_s, car_s, dec_s, cs_s, nc_s, w_s, stage, ins, outs,
     w_sem) = rest[-19:]
    f32 = jnp.float32
    bf = jnp.bfloat16
    batch = stage.shape[0]
    own, width = br_ref.shape
    dim = HEAD_DIM
    base = 8 - (CONV - 1)

    def fetch(b):
        return pltpu.make_async_copy(mem_ref.at[layer, b], stage.at[b], ins.at[b])

    def store(b):
        return pltpu.make_async_copy(stage.at[b], newmem_ref.at[layer, b], outs.at[b])

    maps = [
        pltpu.make_async_copy(w_ref.at[layer], w_s.at[i], w_sem.at[i])
        for i, w_ref in enumerate((wq_ref, wk_ref, wv_ref))
    ]
    for cp in maps:
        cp.start()

    @pl.loop(0, batch)
    def _(b):
        fetch(b).start()

    r = lax.broadcasted_iota(jnp.int32, (own, own), 0)
    c = lax.broadcasted_iota(jnp.int32, (own, own), 1)
    row = lax.broadcasted_iota(jnp.int32, (own, batch), 0)
    seq = lax.broadcasted_iota(jnp.int32, (own, batch), 1)
    belongs = (row // steps) == seq
    closing = row == seq * steps + (steps - 1)
    nt = (((1,), (1,)), ((), ()))
    spread = jnp.where(belongs, 1.0, 0.0)
    counts = jnp.broadcast_to(cvec_ref[...].astype(f32), (8, batch))
    count_row = lax.dot_general(counts, spread, nt, preferred_element_type=f32)[0:1, :]
    count_col = jnp.sum(jnp.where(belongs, counts[0:1, :], 0.0), axis=1, keepdims=True)
    branch = br_ref[...]
    pad_s[:, 8:8 + steps, :] = branch.astype(f32).reshape(batch, steps, width)
    for j in range(CONV - 1):
        rows = st_ref[layer, j].astype(f32)
        for b in range(batch):
            pad_s[b, base + j:base + j + 1, :] = rows[b:b + 1, :]
    total = pad_s[:, base:base + steps, :] * cw_ref[layer, 0:1, :]
    for j in range(1, CONV):
        total = total + pad_s[:, base + j:base + j + steps, :] * cw_ref[layer, j:j + 1, :]
    conv = (total * jax.nn.sigmoid(total)).astype(bf).reshape(own, width)
    conv_s[...] = conv
    for b in range(batch):
        for i in range(CONV - 1):
            nc_s[i, b:b + 1, :] = pad_s[b, pl.ds(base + i + cnt_ref[b], 1), :]
    nc_ref[layer] = nc_s[...].astype(bf)
    for l in range(nc_ref.shape[0]):
        if l != layer and len(rest) > 19:
            nc_ref[l] = rest[1][l]
            nmax_ref[l] = rest[2][l]
        elif l != layer:
            nc_ref[l] = jnp.zeros_like(nc_ref[l])
            nmax_ref[l] = jnp.zeros_like(nmax_ref[l])

    same = (r // steps) == (c // steps)
    causal = same & (r >= c)
    behind = same & (r <= c)
    live_col = (r[:, 0:1] % steps).astype(f32) < count_col
    live_row = (c[0:1, :] % steps).astype(f32) < count_row
    for cp in maps:
        cp.wait()
    for h in range(heads):
        sl = slice(h * dim, (h + 1) * dim)
        q = jnp.dot(conv[:, sl], w_s[0, h], preferred_element_type=f32).astype(bf)
        k = jnp.dot(conv[:, sl], w_s[1, h], preferred_element_type=f32).astype(bf)
        v = jnp.dot(branch[:, sl], w_s[2, h], preferred_element_type=f32).astype(bf)
        cols = []
        rows = []
        for g_ref in (wi_ref, wf_ref):
            col = None
            for i, part in enumerate((q, k, v)):
                w = g_ref[layer, :, i * dim:(i + 1) * dim]
                if heads == 1:
                    w = jnp.broadcast_to(w.astype(f32), (8, dim)).astype(bf)
                one = lax.dot_general(part, w, nt, preferred_element_type=f32)
                two = lax.dot_general(w, part, nt, preferred_element_type=f32)
                col, line = (one, two) if col is None else (col + one, line + two)
            cols.append(col[:, h:h + 1])
            rows.append(line[h:h + 1, :])
        bias_i = bi_ref[layer, h]
        bias_f = bf_ref[layer, h]

        def log_sig(x):
            return jnp.minimum(x, 0.0) - jnp.log1p(jnp.exp(-jnp.abs(x)))

        ig_col = jnp.where(live_col, cols[0] + bias_i, very_negative)
        ig_row = jnp.where(live_row, rows[0] + bias_i, very_negative)
        fg_col = jnp.where(live_col, log_sig(cols[1] + bias_f), 0.0)
        fg_row = jnp.where(live_row, log_sig(rows[1] + bias_f), 0.0)
        cum_col = jnp.sum(jnp.where(causal, fg_row, 0.0), axis=1, keepdims=True)
        end_col = jnp.sum(jnp.where(same, fg_row, 0.0), axis=1, keepdims=True)
        cum_row = jnp.sum(jnp.where(behind, fg_col, 0.0), axis=0, keepdims=True)
        lift_row = ig_row - cum_row
        logw = jnp.where(causal, cum_col + lift_row, very_negative)
        old_max = jnp.sum(jnp.where(belongs, mrow_ref[layer, h:h + 1, :], 0.0), axis=1, keepdims=True)
        carried = cum_col + old_max
        stab = jnp.maximum(jnp.max(logw, axis=1, keepdims=True), carried)
        weights = jnp.exp(logw - stab)
        top = jnp.max(jnp.where(same, end_col + lift_row, very_negative), axis=1, keepdims=True)
        new_max = jnp.maximum(top, end_col + old_max)
        update = jnp.exp(end_col - cum_col + ig_col - new_max)
        nmax_ref[layer, h:h + 1, :] = jnp.sum(jnp.where(closing, new_max, 0.0), axis=0, keepdims=True)
        dec_s[:, h:h + 1] = jnp.exp(end_col + old_max - new_max)
        cs_s[:, h:h + 1] = jnp.exp(carried - stab)
        scores = lax.dot_general(q, k, nt, preferred_element_type=f32)
        scores = (jnp.where(causal, scores, 0.0) * (dim ** -0.5) * weights).astype(bf)
        num_s[:, sl] = jnp.dot(scores, v, preferred_element_type=f32)
        q_s[:, sl] = q.astype(f32)
        k_s[:, sl] = k.astype(f32) * (dim ** -0.5) * update
        v_s[:, sl] = v.astype(f32)

    @pl.loop(0, batch)
    def _(b):
        fetch(b).wait()
        rows = pl.ds(pl.multiple_of(b * steps, 8), steps)
        for h in range(heads):
            sl = slice(h * dim, (h + 1) * dim)
            old = stage[b, h]
            car_s[rows, sl] = jnp.dot(q_s[rows, sl].astype(bf), old.astype(bf), preferred_element_type=f32)
            outer = lax.dot_general(
                k_s[rows, sl].astype(bf), v_s[rows, sl].astype(bf), (((0,), (0,)), ((), ())),
                preferred_element_type=f32,
            )
            stage[b, h] = dec_s[rows, :][0:1, h:h + 1] * old + outer
        store(b).start()

    counts = jnp.broadcast_to(cvec_ref[...].astype(f32), (8, batch))
    row = lax.broadcasted_iota(jnp.int32, (own, batch), 0)
    seq = lax.broadcasted_iota(jnp.int32, (own, batch), 1)
    count_col = jnp.sum(jnp.where((row // steps) == seq, counts[0:1, :], 0.0), axis=1, keepdims=True)
    live = (lax.broadcasted_iota(jnp.int32, (own, 1), 0) % steps).astype(f32) < count_col
    for h in range(heads):
        sl = slice(h * dim, (h + 1) * dim)
        num = num_s[:, sl] + cs_s[:, h:h + 1] * car_s[:, sl]
        centered = num - jnp.mean(num, axis=1, keepdims=True)
        normal = centered * lax.rsqrt(jnp.mean(centered * centered, axis=1, keepdims=True) + epsilon)
        gate = gt_ref[:, sl].astype(f32)
        mixed = normal * og_ref[layer, h:h + 1, :] + sg_ref[layer:layer + 1, sl] * conv_s[:, sl].astype(f32)
        mixed = mixed * (gate * jax.nn.sigmoid(gate))
        mixed_ref[:, sl] = jnp.where(live, mixed, 0.0).astype(bf)
    for b in range(batch):
        store(b).wait()


def memory_cell(layer, steps, counts, bias_input, bias_forget, branch, gate, old_max, state, conv_weight,
                w_input_gate, w_forget_gate, out_gain, skip_gain, w_query, w_key, w_value, memory, previous):
    layers, batch, heads, dim, _ = memory.shape
    own, width = branch.shape
    f32 = jnp.float32
    smem = pl.BlockSpec(memory_space=pltpu.SMEM)
    anyspace = pl.BlockSpec(memory_space=pl.ANY)
    args = [counts, bias_input, bias_forget, counts[None, :], branch, gate, old_max, state, conv_weight,
            w_input_gate, w_forget_gate, out_gain, skip_gain, w_query, w_key, w_value, memory]
    specs = [smem] * 3 + [VM] * 10 + [anyspace] * 4
    aliases = {}
    if previous is not None:
        aliases = {len(args): 2}
        args += list(previous)
        specs += [anyspace, VM, VM]
    big = pltpu.VMEM((own, width), f32)
    small = pltpu.VMEM((own, 128), f32)
    return pl.pallas_call(
        functools.partial(cell_kernel, layer, heads, steps),
        out_shape=(
            jax.ShapeDtypeStruct((own, width), jnp.bfloat16),
            jax.ShapeDtypeStruct((layers, CONV - 1, batch, width), jnp.bfloat16),
            jax.ShapeDtypeStruct(memory.shape, f32),
            jax.ShapeDtypeStruct((layers, heads, batch), f32),
        ),
        in_specs=specs,
        out_specs=(VM, VM, anyspace, VM),
        scratch_shapes=[
            pltpu.VMEM((batch, 8 + steps, width), f32),
            pltpu.VMEM((own, width), jnp.bfloat16),
            big, big, big, big, big, small, small,
            pltpu.VMEM((CONV - 1, batch, width), f32),
            pltpu.VMEM((3, heads, dim, dim), jnp.bfloat16),
            pltpu.VMEM((batch, heads, dim, dim), f32),
            pltpu.SemaphoreType.DMA((batch,)), pltpu.SemaphoreType.DMA((batch,)),
            pltpu.SemaphoreType.DMA((3,)),
        ],
        input_output_aliases=aliases,
        compiler_params=pltpu.CompilerParams(vmem_limit_bytes=FULL_VMEM),
        name="memory_cell",
    )(*args)


def per_device(tokens, live_counts, norm_gain, w_branch, w_silu_gate, conv_weight, w_query, w_key,
               w_value, w_input_gate, w_forget_gate, bias_input, bias_forget, out_gain, skip_gain,
               w_out, conv_state, memory, max_state):
    ndp = lax.axis_size("dp")
    ntp = lax.axis_size("tp")
    steps, features = tokens.shape[1:]
    own = live_counts.shape[0] * steps
    lanes = -(-own // 128) * 128
    chunks = 4 if own % 64 == 0 else 1
    stream = tokens.reshape(ndp, chunks, own // chunks, features)
    old_max = jnp.transpose(max_state, (0, 2, 1))
    states = jnp.transpose(conv_state, (0, 2, 1, 3))
    link = functools.partial(bridge, ndp, ntp, lanes)
    inputs = dict(gain=norm_gain, w_branch=w_branch, w_gate=w_silu_gate)

    branch, gate = link("enter", 0, FULL_VMEM, stream, li=0, **inputs)
    previous = None
    for l in range(LAYERS):
        mixed, new_conv, new_memory, new_max = memory_cell(
            l, steps, live_counts, bias_input, bias_forget, branch, gate, old_max, states, conv_weight,
            w_input_gate, w_forget_gate, out_gain, skip_gain, w_query, w_key, w_value, memory, previous
        )
        previous = (new_memory, new_conv, new_max)
        if l + 1 < LAYERS:
            stream, branch, gate = link(
                f"bridge{l}", l + 1, FULL_VMEM, stream, lo=l, li=l + 1, mixed=mixed, w_out=w_out, **inputs
            )
        else:
            (stream,) = link("leave", l + 1, LEAVE_VMEM, stream, lo=l, mixed=mixed, w_out=w_out)
    return (stream.reshape(tokens.shape), jnp.transpose(new_conv, (0, 2, 1, 3)), new_memory,
            jnp.transpose(new_max, (0, 2, 1)))


def solution(mesh):
    in_specs = (
        P("grp", None, "dp"),
        P(("grp", "dp")),
        P(None, "dp"),
        P(None, "dp", "tp"),
        P(None, "dp", "tp"),
        P(None, None, "tp"),
        P(None, "tp", None, None),
        P(None, "tp", None, None),
        P(None, "tp", None, None),
        P(None, "tp", None),
        P(None, "tp", None),
        P(None, "tp"),
        P(None, "tp"),
        P(None, "tp", None),
        P(None, "tp"),
        P(None, "tp", "dp"),
        P(None, ("grp", "dp"), None, "tp"),
        P(None, ("grp", "dp"), "tp", None, None),
        P(None, ("grp", "dp"), "tp"),
    )
    out_specs = (
        P("grp", None, "dp"),
        P(None, ("grp", "dp"), None, "tp"),
        P(None, ("grp", "dp"), "tp", None, None),
        P(None, ("grp", "dp"), "tp"),
    )
    return jax.shard_map(
        per_device, mesh=mesh, in_specs=in_specs, out_specs=out_specs, check_vma=False
    )
```

time: 137 us -> 113 us (0.82)
  Pallas kernels: 124 us -> 110 us
  local copies, waits for them, and re-layouts: 8.52 us -> 1.75 us
  other arithmetic: 3.41 us -> 0 us
    pallas_call x5, Pallas kernels: 124 us -> 110 us  [the longest x3 83 us: bridge(): pl.pallas_call(functools.partial(bridge_kernel, ndp, ntp, do_out, do_in,...]
    slice x5 -> x0, local copies, waits for them, and re-layouts: 2.42 us -> none  [the longest x2 1.55 us: per_device(): max_list.append(new_max[:, :heads])]
    another operation x4 -> x0, local copies, waits for them, and re-layouts: 2.25 us -> none  [the longest x2 1.45 us: per_device(): jnp.stack([w_input_gate, w_forget_gate], axis=2)]
    broadcast_in_dim x3 -> x0, local copies, waits for them, and re-layouts: 1.98 us -> none  [the longest x2 1.25 us: per_device(): old_max = jnp.repeat(max_state, steps, axis=1)]
    transpose x1 -> x0, other arithmetic: 1.59 us -> none  [per_device(): new_conv = jnp.transpose(jnp.stack(conv_list), (0, 2, 1, 3))]
where the time goes in v3:
time: 113 us
  Pallas kernels  110 us (97%)
  local copies, waits for them, and re-layouts  1.75 us (2%)
    pallas_call x3, Pallas kernels, bridge(): pl.pallas_call(functools.partial(bridge_kernel, ndp, ntp, do_out, do_in,...  83 us
    pallas_call x2, Pallas kernels, memory_cell(): pl.pallas_call(functools.partial(cell_kernel, layer, heads, steps), out_s...  27.3 us

profile of v3, /device:TPU:0, one launch (start us, length us, event | category | flops | bytes accessed | tf_op | source)
XLA Modules:
  0.0 112.8 jit_solution(18106937604166362414)
XLA Ops:
  0.6 20.7 %enter.1 = (bf16[128,1024]{1,0:T(8,128)(2,1)}, bf16[128,1024]{1,0:T(8,128)(2,1)}) custom-call(bf16[4,4,32,512]{3,2,1,0:T(8,128)(2,1)} %bitcast.11, f32[2,512]{1,0:T(2,128)} %refs_3_.3, bf16[2,512,1024]{2,1,0:T(8,128)(2,1)} %refs_4_.1, bf16[2,512,1024]{2,1,0:T(8,128)(2,1)} %refs_5_.1), custom_call_target="tpu_custom_call" | custom-call | tf_op jit(solution)/shard_map/enter/pallas_call | solution.py:445
  21.4 13.5 %memory_cell.2 = (bf16[128,1024]{1,0:T(8,128)(2,1)}, bf16[2,3,16,1024]{3,2,1,0:T(8,128)(2,1)}, f32[2,16,4,256,256]{4,3,2,1,0:T(8,128)}, f32[2,4,16]{2,1,0:T(4,128)}) custom-call(s32[16]{0:T(128)} %cnt_ref.3, f32[2,4]{1,0:T(2,128)} %bi_ref.3, f32[2,4]{1,0:T(2,128)} %bf_ref.3, s32[1,16]{1,0:T(1,128)} %bitcast.18, bf16[128,1024]{1,0:T(8,128)(2,1)} %get-tuple-element.17.br_ref, ...), custom_call_target="tpu_custom_call" | custom-call | tf_op jit(solution)/shard_map/memory_cell/pallas_call | solution.py:628
  34.9 39.0 %bridge0.1 = (bf16[4,4,32,512]{3,2,1,0:T(8,128)(2,1)}, bf16[128,1024]{1,0:T(8,128)(2,1)}, bf16[128,1024]{1,0:T(8,128)(2,1)}) custom-call(bf16[4,4,32,512]{3,2,1,0:T(8,128)(2,1)} %bitcast.12, bf16[4,32,1024]{2,1,0:T(8,128)(2,1)} %bitcast.15, bf16[2,1024,512]{2,1,0:T(8,128)(2,1)} %refs_2_.5, f32[2,512]{1,0:T(2,128)} %refs_3_.3, bf16[2,512,1024]{2,1,0:T(8,128)(2,1)} %refs_4_.1, ...), custom_call_target="tpu_custom_call" | custom-call | tf_op jit(solution)/shard_map/bridge0/pallas_call | solution.py:445
  73.9 0.0 copy-start
  73.9 0.0 copy-start.1
  73.9 13.8 %memory_cell.3 = (bf16[128,1024]{1,0:T(8,128)(2,1)}, bf16[2,3,16,1024]{3,2,1,0:T(8,128)(2,1)}, f32[2,16,4,256,256]{4,3,2,1,0:T(8,128)}, f32[2,4,16]{2,1,0:T(4,128)}) custom-call(s32[16]{0:T(128)} %cnt_ref.3, f32[2,4]{1,0:T(2,128)} %bi_ref.3, f32[2,4]{1,0:T(2,128)} %bf_ref.3, s32[1,16]{1,0:T(1,128)} %bitcast.19, ...), custom_call_target="tpu_custom_call", output_to_operand_aliasing={{2}: (17, {})} | custom-call | tf_op jit(solution)/shard_map/memory_cell/pallas_call | solution.py:628
  87.7 0.0 copy-done
  87.7 0.0 copy-done.1
  87.7 0.0 copy-start.2
  87.7 0.9 copy-done.2
  88.6 23.3 %leave.1 = bf16[4,4,32,512]{3,2,1,0:T(8,128)(2,1)S(1)} custom-call(bf16[4,4,32,512]{3,2,1,0:T(8,128)(2,1)S(1)} %copy-done.1, bf16[4,32,1024]{2,1,0:T(8,128)(2,1)S(1)} %bitcast.10, bf16[2,1024,512]{2,1,0:T(8,128)(2,1)S(1)} %copy-done), custom_call_target="tpu_custom_call" | custom-call | tf_op jit(solution)/shard_map/leave/pallas_call | solution.py:445
  112.0 0.8 copy.26
Async XLA Ops:
  73.9 13.8 %copy-start = (bf16[2,1024,512]{2,1,0:T(8,128)(2,1)S(1)}, bf16[2,1024,512]{2,1,0:T(8,128)(2,1)}, u32[]{:S(2)}) copy-start(bf16[2,1024,512]{2,1,0:T(8,128)(2,1)} %refs_2_.5) | copy-start | bytes 6291460
  73.9 13.8 %copy-start.1 = (bf16[4,4,32,512]{3,2,1,0:T(8,128)(2,1)S(1)}, bf16[4,4,32,512]{3,2,1,0:T(8,128)(2,1)}, u32[]{:S(2)}) copy-start(bf16[4,4,32,512]{3,2,1,0:T(8,128)(2,1)} %get-tuple-element.20.refs_0_) | copy-start | bytes 1572868
  87.7 1.0 copy-start.2

commit v4 on v3

--- a/solution.py
+++ b/solution.py
@@ -37,7 +37,7 @@
     x = me // 2
     partner = me + 1 - 2 * core
     z = lax.axis_index("tp")
-    tok = R["tok"]
+    tok = R["tok_s"]
     chunks, piece, feats = tok.shape[1:]
     own = chunks * piece
     halves = 2 if chunks > 1 else 1
@@ -49,9 +49,16 @@
     def load(name, layer):
         return pltpu.make_async_copy(R[name].at[layer], R[name + "_s"], R[name + "_m"])
 
+    def bring(name):
+        return pltpu.make_async_copy(R[name], R[name + "_s"], R[name + "_m"])
+
+    for name in ("m", "tok") if do_out else ("tok", "gain"):
+        bring(name).start()
     wanted = ([("wo", lo)] if do_out else []) + ([("wb", li), ("wg", li)] if do_in else [])
     for name, layer in wanted:
         load(name, layer).start()
+    if do_out and do_in:
+        bring("gain").start()
     barrier = pltpu.get_barrier_semaphore()
     for off in range(1, ndp):
         pl.semaphore_signal(barrier, inc=1, device_id={"dp": (me + off) % ndp}, device_id_type=MESH)
@@ -65,6 +72,8 @@
         def _():
             pl.semaphore_signal(barrier, inc=1, device_id={"tp": z + 1}, device_id_type=MESH)
         greeted = greeted + jnp.where(z > 0, 1, 0) + jnp.where(z < ntp - 1, 1, 0)
+    if do_out:
+        bring("m").wait()
     pl.semaphore_wait(barrier, greeted)
 
     def ahead(g):
@@ -83,7 +92,7 @@
         groups = [(kind, g, h) for g in range(nx) for h in range(halves) for kind in ("other", "mine")]
 
     if do_out:
-        m_ref, got, psum = R["m"], R["got"], R["psum"]
+        m_ref, got, psum = R["m_s"], R["got"], R["psum"]
         width = m_ref.shape[2]
         fresh = R["fresh"]
 
@@ -110,6 +119,7 @@
         for c in range(chunks):
             near(c).start()
         load("wo", lo).wait()
+        bring("tok").wait()
 
         def rows_of(kind, g, h):
             if g == nx - 1:
@@ -215,7 +225,7 @@
             else:
                 aux_s[d, 0:1, :own] += line
             done.append((kind, gw))
-            scaled = (rows * R["gain"][li:li + 1, :]).astype(bf)
+            scaled = (rows * R["gain_s"][li:li + 1, :]).astype(bf)
             for k in range(2):
                 part = jnp.dot(scaled, weights[k][...], preferred_element_type=f32).astype(bf)
                 part = part.reshape(step, piece, wide)
@@ -243,6 +253,9 @@
                 forward(*waiting.pop(0))
 
     if do_in:
+        bring("gain").wait()
+        if not do_out:
+            bring("tok").wait()
         for name in ("wb", "wg"):
             load(name, li).wait()
     if not do_out:
@@ -303,7 +316,7 @@
             @pl.when(center)
             def _():
                 done, waiting = [], []
-                lag = 3
+                lag = 4
                 for p in range(spots + lag):
                     if p < spots:
                         if p % step == 0:
@@ -331,6 +344,9 @@
                 across(g, c).wait_send()
                 passed(g, c).wait_send()
 
+    if do_out and do_in:
+        keep = pltpu.make_async_copy(fresh, R["fresh_o"], R["fresh_m"])
+        keep.start()
     if do_in:
         last = nx - 1
         for g in range(nx):
@@ -355,6 +371,8 @@
                     out[c * piece:(c + 1) * piece, :] = (
                         total * inv[c * piece:(c + 1) * piece, :]
                     ).astype(bf)
+        if do_out:
+            keep.wait()
         for g in range(nx):
             for kind in ("mine", "other"):
                 if (kind, g) != ("mine", last):
@@ -386,14 +404,14 @@
         args.append(a)
         specs.append(spec)
 
-    take("tok", tok)
+    take("tok", tok, weight)
     if do_out:
         width = mixed.shape[-1]
-        take("m", mixed.reshape(chunks, piece, width))
+        take("m", mixed.reshape(chunks, piece, width), weight)
         take("wo", w_out, weight)
     if do_in:
         width = w_branch.shape[-1]
-        take("gain", gain)
+        take("gain", gain, weight)
         take("wb", w_branch, weight)
         take("wg", w_gate, weight)
 
@@ -402,7 +420,7 @@
         outs.append(jax.ShapeDtypeStruct(shape, dtype))
 
     if do_out:
-        give("fresh", tok.shape, bf)
+        give("fresh_o" if do_in else "fresh", tok.shape, bf)
     if do_in:
         give("ob", (own, width), bf)
         give("og", (own, width), bf)
@@ -419,7 +437,17 @@
         flag(key + "_s", *shape)
         flag(key + "_r", *shape)
 
+    room("tok_s", tok.shape, bf)
+    flag("tok_m")
+    if do_in:
+        room("gain_s", gain.shape, f32)
+        flag("gain_m")
     if do_out:
+        room("m_s", (chunks, piece, width), bf)
+        flag("m_m")
+        if do_in:
+            room("fresh", tok.shape, bf)
+            flag("fresh_m")
         room("got", (nx, 2, chunks, piece, width), bf)
         room("psum", (spots, piece, feats), f32)
         room("wo_s", w_out.shape[1:], bf)
@@ -446,7 +474,7 @@
         functools.partial(bridge_kernel, ndp, ntp, do_out, do_in, lo, li, names),
         out_shape=tuple(outs),
         in_specs=specs,
-        out_specs=(VM,) * len(outs),
+        out_specs=((weight, VM, VM) if do_out and do_in else (VM,) * len(outs)),
         scratch_shapes=scratch,
         compiler_params=pltpu.CompilerParams(
             collective_id=cid, has_side_effects=True, vmem_limit_bytes=limit
@@ -455,11 +483,13 @@
     )(*args)
 
 
-def cell_kernel(layer, heads, steps, cnt_ref, bi_ref, bf_ref, cvec_ref, br_ref, gt_ref, mrow_ref, st_ref,
-                cw_ref, wi_ref, wf_ref, og_ref, sg_ref, wq_ref, wk_ref, wv_ref, mem_ref, *rest):
-    (mixed_ref, nc_ref, newmem_ref, nmax_ref,
+def cell_kernel(layer, heads, steps, cnt_any, cvec_any, br_any, gt_any, mrow_any, bi_any, bf_any, st_any,
+                cw_any, wi_any, wf_any, og_any, sg_any, wq_ref, wk_ref, wv_ref, mem_ref, *rest):
+    (mixed_any, nc_any, newmem_ref, nmax_any,
+     cnt_ref, cvec_ref, br_ref, gt_ref, mrow_ref, bi_ref, bf_ref, st_ref, cw_ref, wi_ref, wf_ref, og_ref,
+     sg_ref, mixed_ref, nc_ref, nmax_ref,
      pad_s, conv_s, q_s, k_s, v_s, num_s, car_s, dec_s, cs_s, nc_s, w_s, stage, ins, outs,
-     w_sem) = rest[-19:]
+     w_sem, s_sem, o_sem) = rest[-37:]
     f32 = jnp.float32
     bf = jnp.bfloat16
     batch = stage.shape[0]
@@ -477,12 +507,26 @@
         pltpu.make_async_copy(w_ref.at[layer], w_s.at[i], w_sem.at[i])
         for i, w_ref in enumerate((wq_ref, wk_ref, wv_ref))
     ]
+    smalls = [
+        pltpu.make_async_copy(a, b, s_sem.at[i])
+        for i, (a, b) in enumerate((
+            (br_any, br_ref), (st_any.at[layer], st_ref), (cw_any, cw_ref), (cnt_any, cnt_ref),
+            (cvec_any, cvec_ref), (mrow_any, mrow_ref), (bi_any, bi_ref), (bf_any, bf_ref),
+            (wi_any, wi_ref), (wf_any, wf_ref), (og_any, og_ref), (sg_any, sg_ref), (gt_any, gt_ref),
+        ))
+    ]
+    for cp in smalls[:8]:
+        cp.start()
     for cp in maps:
+        cp.start()
+    for cp in smalls[8:]:
         cp.start()
 
     @pl.loop(0, batch)
     def _(b):
         fetch(b).start()
+    for cp in smalls:
+        cp.wait()
 
     r = lax.broadcasted_iota(jnp.int32, (own, own), 0)
     c = lax.broadcasted_iota(jnp.int32, (own, own), 1)
@@ -498,7 +542,7 @@
     branch = br_ref[...]
     pad_s[:, 8:8 + steps, :] = branch.astype(f32).reshape(batch, steps, width)
     for j in range(CONV - 1):
-        rows = st_ref[layer, j].astype(f32)
+        rows = st_ref[j].astype(f32)
         for b in range(batch):
             pad_s[b, base + j:base + j + 1, :] = rows[b:b + 1, :]
     total = pad_s[:, base:base + steps, :] * cw_ref[layer, 0:1, :]
@@ -509,14 +553,7 @@
     for b in range(batch):
         for i in range(CONV - 1):
             nc_s[i, b:b + 1, :] = pad_s[b, pl.ds(base + i + cnt_ref[b], 1), :]
-    nc_ref[layer] = nc_s[...].astype(bf)
-    for l in range(nc_ref.shape[0]):
-        if l != layer and len(rest) > 19:
-            nc_ref[l] = rest[1][l]
-            nmax_ref[l] = rest[2][l]
-        elif l != layer:
-            nc_ref[l] = jnp.zeros_like(nc_ref[l])
-            nmax_ref[l] = jnp.zeros_like(nmax_ref[l])
+    nc_ref[...] = nc_s[...].astype(bf)
 
     same = (r // steps) == (c // steps)
     causal = same & (r >= c)
@@ -525,14 +562,35 @@
     live_row = (c[0:1, :] % steps).astype(f32) < count_row
     for cp in maps:
         cp.wait()
+    def log_sig(x):
+        return jnp.minimum(x, 0.0) - jnp.log1p(jnp.exp(-jnp.abs(x)))
+
+    def side(columns):
+        lane = lax.broadcasted_iota(jnp.int32, (own, heads), 1)
+        out = jnp.broadcast_to(columns[0], (own, heads))
+        for h in range(1, heads):
+            out = jnp.where(lane == h, columns[h], out)
+        return out
+
+    def pile(lines):
+        level = lax.broadcasted_iota(jnp.int32, (heads, own), 0)
+        out = jnp.broadcast_to(lines[0], (heads, own))
+        for h in range(1, heads):
+            out = jnp.where(level == h, lines[h], out)
+        return out
+
+    exact = lax.Precision.HIGHEST
+    cols = ([], [])
+    lines = ([], [])
     for h in range(heads):
         sl = slice(h * dim, (h + 1) * dim)
         q = jnp.dot(conv[:, sl], w_s[0, h], preferred_element_type=f32).astype(bf)
         k = jnp.dot(conv[:, sl], w_s[1, h], preferred_element_type=f32).astype(bf)
         v = jnp.dot(branch[:, sl], w_s[2, h], preferred_element_type=f32).astype(bf)
-        cols = []
-        rows = []
-        for g_ref in (wi_ref, wf_ref):
+        q_s[:, sl] = q.astype(f32)
+        k_s[:, sl] = k.astype(f32) * (dim ** -0.5)
+        v_s[:, sl] = v.astype(f32)
+        for n, g_ref in enumerate((wi_ref, wf_ref)):
             col = None
             for i, part in enumerate((q, k, v)):
                 w = g_ref[layer, :, i * dim:(i + 1) * dim]
@@ -541,42 +599,54 @@
                 one = lax.dot_general(part, w, nt, preferred_element_type=f32)
                 two = lax.dot_general(w, part, nt, preferred_element_type=f32)
                 col, line = (one, two) if col is None else (col + one, line + two)
-            cols.append(col[:, h:h + 1])
-            rows.append(line[h:h + 1, :])
-        bias_i = bi_ref[layer, h]
-        bias_f = bf_ref[layer, h]
-
-        def log_sig(x):
-            return jnp.minimum(x, 0.0) - jnp.log1p(jnp.exp(-jnp.abs(x)))
-
-        ig_col = jnp.where(live_col, cols[0] + bias_i, very_negative)
-        ig_row = jnp.where(live_row, rows[0] + bias_i, very_negative)
-        fg_col = jnp.where(live_col, log_sig(cols[1] + bias_f), 0.0)
-        fg_row = jnp.where(live_row, log_sig(rows[1] + bias_f), 0.0)
+            cols[n].append(col[:, h:h + 1])
+            lines[n].append(line[h:h + 1, :])
+    bias_col = [ref[layer:layer + 1, :] for ref in (bi_ref, bf_ref)]
+    head_eye = (
+        lax.broadcasted_iota(jnp.int32, (heads, heads), 0) == lax.broadcasted_iota(jnp.int32, (heads, heads), 1)
+    )
+    bias_row = [jnp.sum(jnp.where(head_eye, b, 0.0), axis=1, keepdims=True) for b in bias_col]
+    ig_col = jnp.where(live_col, side(cols[0]) + bias_col[0], very_negative)
+    fg_col = jnp.where(live_col, log_sig(side(cols[1]) + bias_col[1]), 0.0)
+    ig_row = jnp.where(live_row, pile(lines[0]) + bias_row[0], very_negative)
+    fg_row = jnp.where(live_row, log_sig(pile(lines[1]) + bias_row[1]), 0.0)
+    ones = jnp.where(causal, 1.0, 0.0)
+    sames = jnp.where(same, 1.0, 0.0)
+    if heads == 1:
         cum_col = jnp.sum(jnp.where(causal, fg_row, 0.0), axis=1, keepdims=True)
         end_col = jnp.sum(jnp.where(same, fg_row, 0.0), axis=1, keepdims=True)
         cum_row = jnp.sum(jnp.where(behind, fg_col, 0.0), axis=0, keepdims=True)
-        lift_row = ig_row - cum_row
-        logw = jnp.where(causal, cum_col + lift_row, very_negative)
-        old_max = jnp.sum(jnp.where(belongs, mrow_ref[layer, h:h + 1, :], 0.0), axis=1, keepdims=True)
-        carried = cum_col + old_max
-        stab = jnp.maximum(jnp.max(logw, axis=1, keepdims=True), carried)
-        weights = jnp.exp(logw - stab)
-        top = jnp.max(jnp.where(same, end_col + lift_row, very_negative), axis=1, keepdims=True)
-        new_max = jnp.maximum(top, end_col + old_max)
-        update = jnp.exp(end_col - cum_col + ig_col - new_max)
-        nmax_ref[layer, h:h + 1, :] = jnp.sum(jnp.where(closing, new_max, 0.0), axis=0, keepdims=True)
-        dec_s[:, h:h + 1] = jnp.exp(end_col + old_max - new_max)
-        cs_s[:, h:h + 1] = jnp.exp(carried - stab)
-        scores = lax.dot_general(q, k, nt, preferred_element_type=f32)
-        scores = (jnp.where(causal, scores, 0.0) * (dim ** -0.5) * weights).astype(bf)
-        num_s[:, sl] = jnp.dot(scores, v, preferred_element_type=f32)
-        q_s[:, sl] = q.astype(f32)
-        k_s[:, sl] = k.astype(f32) * (dim ** -0.5) * update
-        v_s[:, sl] = v.astype(f32)
-
-    @pl.loop(0, batch)
-    def _(b):
+        old_max = jnp.sum(jnp.where(belongs, mrow_ref[layer], 0.0), axis=1, keepdims=True)
+    else:
+        cum_col = jnp.dot(ones, fg_col, preferred_element_type=f32, precision=exact)
+        end_col = jnp.dot(sames, fg_col, preferred_element_type=f32, precision=exact)
+        cum_row = lax.dot_general(fg_row, ones, nt, preferred_element_type=f32, precision=exact)
+        old_max = lax.dot_general(spread, mrow_ref[layer], nt, preferred_element_type=f32, precision=exact)
+    lift_row = ig_row - cum_row
+    carried = cum_col + old_max
+    tops = []
+    ends_ = []
+    for h in range(heads):
+        lift = lift_row[h:h + 1, :]
+        logw = jnp.where(causal, cum_col[:, h:h + 1] + lift, very_negative)
+        tops.append(jnp.max(logw, axis=1, keepdims=True))
+        ends_.append(jnp.max(jnp.where(same, lift, very_negative), axis=1, keepdims=True))
+    stab = jnp.maximum(side(tops), carried)
+    new_max = jnp.maximum(end_col + side(ends_), end_col + old_max)
+    update = jnp.exp(end_col - cum_col + ig_col - new_max)
+    dec_s[:, :heads] = jnp.exp(end_col + old_max - new_max)
+    cs_s[:, :heads] = jnp.exp(carried - stab)
+    for h in range(heads):
+        sl = slice(h * dim, (h + 1) * dim)
+        logw = jnp.where(causal, cum_col[:, h:h + 1] + lift_row[h:h + 1, :], very_negative)
+        weights = jnp.exp(logw - stab[:, h:h + 1])
+        nmax_ref[h:h + 1, :] = jnp.sum(jnp.where(closing, new_max[:, h:h + 1], 0.0), axis=0, keepdims=True)
+        scores = lax.dot_general(q_s[:, sl].astype(bf), k_s[:, sl].astype(bf), nt, preferred_element_type=f32)
+        scores = (jnp.where(causal, scores, 0.0) * weights).astype(bf)
+        num_s[:, sl] = jnp.dot(scores, v_s[:, sl].astype(bf), preferred_element_type=f32)
+        k_s[:, sl] = k_s[:, sl] * update[:, h:h + 1]
+
+    def advance(b):
         fetch(b).wait()
         rows = pl.ds(pl.multiple_of(b * steps, 8), steps)
         for h in range(heads):
@@ -589,6 +659,13 @@
             )
             stage[b, h] = dec_s[rows, :][0:1, h:h + 1] * old + outer
         store(b).start()
+
+    stride = 2 if batch % 2 == 0 else 1
+
+    @pl.loop(0, batch, step=stride)
+    def _(b):
+        for i in range(stride):
+            advance(b + i)
 
     counts = jnp.broadcast_to(cvec_ref[...].astype(f32), (8, batch))
     row = lax.broadcasted_iota(jnp.int32, (own, batch), 0)
@@ -604,8 +681,18 @@
         mixed = normal * og_ref[layer, h:h + 1, :] + sg_ref[layer:layer + 1, sl] * conv_s[:, sl].astype(f32)
         mixed = mixed * (gate * jax.nn.sigmoid(gate))
         mixed_ref[:, sl] = jnp.where(live, mixed, 0.0).astype(bf)
+    ends = [
+        pltpu.make_async_copy(a, b, o_sem.at[i])
+        for i, (a, b) in enumerate((
+            (mixed_ref, mixed_any), (nc_ref, nc_any.at[layer]), (nmax_ref, nmax_any.at[layer])
+        ))
+    ]
+    for cp in ends:
+        cp.start()
     for b in range(batch):
         store(b).wait()
+    for cp in ends:
+        cp.wait()
 
 
 def memory_cell(layer, steps, counts, bias_input, bias_forget, branch, gate, old_max, state, conv_weight,
@@ -613,16 +700,22 @@
     layers, batch, heads, dim, _ = memory.shape
     own, width = branch.shape
     f32 = jnp.float32
-    smem = pl.BlockSpec(memory_space=pltpu.SMEM)
+    bf = jnp.bfloat16
     anyspace = pl.BlockSpec(memory_space=pl.ANY)
-    args = [counts, bias_input, bias_forget, counts[None, :], branch, gate, old_max, state, conv_weight,
+    args = [counts, counts[None, :], branch, gate, old_max, bias_input, bias_forget, state, conv_weight,
             w_input_gate, w_forget_gate, out_gain, skip_gain, w_query, w_key, w_value, memory]
-    specs = [smem] * 3 + [VM] * 10 + [anyspace] * 4
+    held = [pltpu.SMEM(counts.shape, jnp.int32)]
+    held += [pltpu.VMEM(a.shape[1:] if a is state else a.shape, a.dtype) for a in args[1:13]]
+    held += [
+        pltpu.VMEM((own, width), bf),
+        pltpu.VMEM((CONV - 1, batch, width), bf),
+        pltpu.VMEM((heads, batch), f32),
+    ]
     aliases = {}
     if previous is not None:
-        aliases = {len(args): 2}
+        aliases = {len(args): 2, len(args) + 1: 1, len(args) + 2: 3}
         args += list(previous)
-        specs += [anyspace, VM, VM]
+    specs = [anyspace] * len(args)
     big = pltpu.VMEM((own, width), f32)
     small = pltpu.VMEM((own, 128), f32)
     return pl.pallas_call(
@@ -634,8 +727,8 @@
             jax.ShapeDtypeStruct((layers, heads, batch), f32),
         ),
         in_specs=specs,
-        out_specs=(VM, VM, anyspace, VM),
-        scratch_shapes=[
+        out_specs=(anyspace,) * 4,
+        scratch_shapes=held + [
             pltpu.VMEM((batch, 8 + steps, width), f32),
             pltpu.VMEM((own, width), jnp.bfloat16),
             big, big, big, big, big, small, small,
@@ -643,7 +736,7 @@
             pltpu.VMEM((3, heads, dim, dim), jnp.bfloat16),
             pltpu.VMEM((batch, heads, dim, dim), f32),
             pltpu.SemaphoreType.DMA((batch,)), pltpu.SemaphoreType.DMA((batch,)),
-            pltpu.SemaphoreType.DMA((3,)),
+            pltpu.SemaphoreType.DMA((3,)), pltpu.SemaphoreType.DMA((13,)), pltpu.SemaphoreType.DMA((3,)),
         ],
         input_output_aliases=aliases,
         compiler_params=pltpu.CompilerParams(vmem_limit_bytes=FULL_VMEM),

time: 113 us -> 109 us (0.965)
  Pallas kernels: 110 us -> 106 us
    pallas_call x3, Pallas kernels: 83 us -> 79.8 us  [bridge(): pl.pallas_call(functools.partial(bridge_kernel, ndp, ntp, do_out, do_in,...]
where the time goes in v4:
time: 109 us
  Pallas kernels  106 us (97%)
  local copies, waits for them, and re-layouts  1.75 us (2%)
    pallas_call x3, Pallas kernels, bridge(): pl.pallas_call(functools.partial(bridge_kernel, ndp, ntp, do_out, do_in,...  79.8 us
    pallas_call x2, Pallas kernels, memory_cell(): pl.pallas_call(functools.partial(cell_kernel, layer, heads, steps), out_s...  26.6 us

profile of v4, /device:TPU:0, one launch (start us, length us, event | category | flops | bytes accessed | tf_op | source)
XLA Modules:
  0.0 108.8 jit_solution(18435432858929614399)
XLA Ops:
  0.6 19.9 %enter.1 = (bf16[128,1024]{1,0:T(8,128)(2,1)}, bf16[128,1024]{1,0:T(8,128)(2,1)}) custom-call(bf16[4,4,32,512]{3,2,1,0:T(8,128)(2,1)} %bitcast.11, f32[2,512]{1,0:T(2,128)} %refs_3_.3, bf16[2,512,1024]{2,1,0:T(8,128)(2,1)} %refs_4_.1, bf16[2,512,1024]{2,1,0:T(8,128)(2,1)} %refs_5_.1), custom_call_target="tpu_custom_call" | custom-call | tf_op jit(solution)/shard_map/enter/pallas_call | solution.py:473
  20.5 13.2 %memory_cell.2 = (bf16[128,1024]{1,0:T(8,128)(2,1)}, bf16[2,3,16,1024]{3,2,1,0:T(8,128)(2,1)}, f32[2,16,4,256,256]{4,3,2,1,0:T(8,128)}, f32[2,4,16]{2,1,0:T(4,128)}) custom-call(s32[16]{0:T(128)} %cnt_any.3, s32[1,16]{1,0:T(1,128)} %bitcast.19, bf16[128,1024]{1,0:T(8,128)(2,1)} %get-tuple-element.17.br_any, bf16[128,1024]{1,0:T(8,128)(2,1)} %get-tuple-element.18.gt_any, ...), custom_call_target="tpu_custom_call" | custom-call | tf_op jit(solution)/shard_map/memory_cell/pallas_call | solution.py:721
  33.8 37.0 %bridge0.1 = (bf16[4,4,32,512]{3,2,1,0:T(8,128)(2,1)}, bf16[128,1024]{1,0:T(8,128)(2,1)}, bf16[128,1024]{1,0:T(8,128)(2,1)}) custom-call(bf16[4,4,32,512]{3,2,1,0:T(8,128)(2,1)} %bitcast.12, bf16[4,32,1024]{2,1,0:T(8,128)(2,1)} %bitcast.15, bf16[2,1024,512]{2,1,0:T(8,128)(2,1)} %refs_2_.5, f32[2,512]{1,0:T(2,128)} %refs_3_.3, bf16[2,512,1024]{2,1,0:T(8,128)(2,1)} %refs_4_.1, ...), custom_call_target="tpu_custom_call" | custom-call | tf_op jit(solution)/shard_map/bridge0/pallas_call | solution.py:473
  70.8 0.0 copy-start
  70.8 0.0 copy-start.1
  70.8 13.3 %memory_cell.3 = (bf16[128,1024]{1,0:T(8,128)(2,1)}, bf16[2,3,16,1024]{3,2,1,0:T(8,128)(2,1)}, f32[2,16,4,256,256]{4,3,2,1,0:T(8,128)}, f32[2,4,16]{2,1,0:T(4,128)}) custom-call(s32[16]{0:T(128)} %cnt_any.3, s32[1,16]{1,0:T(1,128)} %bitcast.20, ...), custom_call_target="tpu_custom_call", output_to_operand_aliasing={{2}: (17, {}), {1}: (18, {}), {3}: (19, {})} | custom-call | tf_op jit(solution)/shard_map/memory_cell/pallas_call | solution.py:721
  84.2 0.0 copy-done
  84.2 0.0 copy-done.1
  84.2 0.0 copy-start.2
  84.2 0.9 copy-done.2
  85.2 22.9 %leave.1 = bf16[4,4,32,512]{3,2,1,0:T(8,128)(2,1)S(1)} custom-call(bf16[4,4,32,512]{3,2,1,0:T(8,128)(2,1)S(1)} %copy-done.1, bf16[4,32,1024]{2,1,0:T(8,128)(2,1)S(1)} %bitcast.10, bf16[2,1024,512]{2,1,0:T(8,128)(2,1)S(1)} %copy-done), custom_call_target="tpu_custom_call" | custom-call | tf_op jit(solution)/shard_map/leave/pallas_call | solution.py:473
  108.1 0.8 copy.30
Async XLA Ops:
  70.8 13.4 %copy-start = (bf16[2,1024,512]{2,1,0:T(8,128)(2,1)S(1)}, bf16[2,1024,512]{2,1,0:T(8,128)(2,1)}, u32[]{:S(2)}) copy-start(bf16[2,1024,512]{2,1,0:T(8,128)(2,1)} %refs_2_.5) | copy-start | bytes 6291460
  70.8 13.4 %copy-start.1 = (bf16[4,4,32,512]{3,2,1,0:T(8,128)(2,1)S(1)}, bf16[4,4,32,512]{3,2,1,0:T(8,128)(2,1)}, u32[]{:S(2)}) copy-start(bf16[4,4,32,512]{3,2,1,0:T(8,128)(2,1)} %get-tuple-element.20.refs_0_) | copy-start | bytes 1572868
  84.2 1.0 copy-start.2

commit v5 on v4

--- a/solution.py
+++ b/solution.py
@@ -303,6 +303,8 @@
                                 @pl.when(inner)
                                 def _():
                                     down(p).start()
+                            if do_in:
+                                flush(waiting)
                         finish(i, done, waiting)
                     if do_in:
                         flush(waiting)
@@ -323,6 +325,8 @@
                             product_out(p // step)
                         zsum[p] = (gathered(p) if ntp > 2 else psum[p]).astype(bf)
                         cross(p).start()
+                    if do_in:
+                        flush(waiting)
                     q = p - lag
                     if q >= 0:
                         cross(q).wait_recv()

time: 109 us -> 109 us (level)
  no operation moved by 1% of the time
where the time goes in v5:
time: 109 us
  Pallas kernels  106 us (97%)
  local copies, waits for them, and re-layouts  1.75 us (2%)
    pallas_call x3, Pallas kernels, bridge(): pl.pallas_call(functools.partial(bridge_kernel, ndp, ntp, do_out, do_in,...  79.9 us
    pallas_call x2, Pallas kernels, memory_cell(): pl.pallas_call(functools.partial(cell_kernel, layer, heads, steps), out_s...  26.6 us

profile of v5, /device:TPU:0, one launch (start us, length us, event | category | flops | bytes accessed | tf_op | source)
XLA Modules:
  0.0 108.9 jit_solution(15385805846653437511)
XLA Ops:
  0.6 19.9 %enter.1 = (bf16[128,1024]{1,0:T(8,128)(2,1)}, bf16[128,1024]{1,0:T(8,128)(2,1)}) custom-call(bf16[4,4,32,512]{3,2,1,0:T(8,128)(2,1)} %bitcast.11, f32[2,512]{1,0:T(2,128)} %refs_3_.3, bf16[2,512,1024]{2,1,0:T(8,128)(2,1)} %refs_4_.1, bf16[2,512,1024]{2,1,0:T(8,128)(2,1)} %refs_5_.1), custom_call_target="tpu_custom_call" | custom-call | tf_op jit(solution)/shard_map/enter/pallas_call | solution.py:477
  20.5 13.2 %memory_cell.2 = (bf16[128,1024]{1,0:T(8,128)(2,1)}, bf16[2,3,16,1024]{3,2,1,0:T(8,128)(2,1)}, f32[2,16,4,256,256]{4,3,2,1,0:T(8,128)}, f32[2,4,16]{2,1,0:T(4,128)}) custom-call(s32[16]{0:T(128)} %cnt_any.3, s32[1,16]{1,0:T(1,128)} %bitcast.19, bf16[128,1024]{1,0:T(8,128)(2,1)} %get-tuple-element.17.br_any, bf16[128,1024]{1,0:T(8,128)(2,1)} %get-tuple-element.18.gt_any, ...), custom_call_target="tpu_custom_call" | custom-call | tf_op jit(solution)/shard_map/memory_cell/pallas_call | solution.py:725
  33.8 36.7 %bridge0.1 = (bf16[4,4,32,512]{3,2,1,0:T(8,128)(2,1)}, bf16[128,1024]{1,0:T(8,128)(2,1)}, bf16[128,1024]{1,0:T(8,128)(2,1)}) custom-call(bf16[4,4,32,512]{3,2,1,0:T(8,128)(2,1)} %bitcast.12, bf16[4,32,1024]{2,1,0:T(8,128)(2,1)} %bitcast.15, bf16[2,1024,512]{2,1,0:T(8,128)(2,1)} %refs_2_.5, f32[2,512]{1,0:T(2,128)} %refs_3_.3, bf16[2,512,1024]{2,1,0:T(8,128)(2,1)} %refs_4_.1, ...), custom_call_target="tpu_custom_call" | custom-call | tf_op jit(solution)/shard_map/bridge0/pallas_call | solution.py:477
  70.5 0.0 copy-start
  70.5 0.0 copy-start.1
  70.5 13.3 %memory_cell.3 = (bf16[128,1024]{1,0:T(8,128)(2,1)}, bf16[2,3,16,1024]{3,2,1,0:T(8,128)(2,1)}, f32[2,16,4,256,256]{4,3,2,1,0:T(8,128)}, f32[2,4,16]{2,1,0:T(4,128)}) custom-call(s32[16]{0:T(128)} %cnt_any.3, s32[1,16]{1,0:T(1,128)} %bitcast.20, ...), custom_call_target="tpu_custom_call", output_to_operand_aliasing={{2}: (17, {}), {1}: (18, {}), {3}: (19, {})} | custom-call | tf_op jit(solution)/shard_map/memory_cell/pallas_call | solution.py:725
  83.9 0.0 copy-done
  83.9 0.0 copy-done.1
  83.9 0.0 copy-start.2
  83.9 0.9 copy-done.2
  84.9 23.2 %leave.1 = bf16[4,4,32,512]{3,2,1,0:T(8,128)(2,1)S(1)} custom-call(bf16[4,4,32,512]{3,2,1,0:T(8,128)(2,1)S(1)} %copy-done.1, bf16[4,32,1024]{2,1,0:T(8,128)(2,1)S(1)} %bitcast.10, bf16[2,1024,512]{2,1,0:T(8,128)(2,1)S(1)} %copy-done), custom_call_target="tpu_custom_call" | custom-call | tf_op jit(solution)/shard_map/leave/pallas_call | solution.py:477
  108.1 0.8 copy.30
Async XLA Ops:
  70.5 13.4 %copy-start = (bf16[2,1024,512]{2,1,0:T(8,128)(2,1)S(1)}, bf16[2,1024,512]{2,1,0:T(8,128)(2,1)}, u32[]{:S(2)}) copy-start(bf16[2,1024,512]{2,1,0:T(8,128)(2,1)} %refs_2_.5) | copy-start | bytes 6291460
  70.5 13.4 %copy-start.1 = (bf16[4,4,32,512]{3,2,1,0:T(8,128)(2,1)S(1)}, bf16[4,4,32,512]{3,2,1,0:T(8,128)(2,1)}, u32[]{:S(2)}) copy-start(bf16[4,4,32,512]{3,2,1,0:T(8,128)(2,1)} %get-tuple-element.20.refs_0_) | copy-start | bytes 1572868
  83.9 1.0 copy-start.2
